TPU v7x, 256 devices: a whole 4x4x8 slice. The times are simulated.
256 devices in a mesh: fs: 16 (over y, x), tp: 16 (over z, core).
Axes of the slice: x: 4, y: 4, z: 8, core: 2. Of those that a mesh axis runs over, the one named last changes fastest.
Arguments:
- tokens_in: bfloat16 [65536, 2048], P(('fs', 'tp')), may hold values from -6 to 6
- gate_cotangent: bfloat16 [65536, 1024], P(('fs', 'tp')), may hold values from -0.09375 to 0.09375
- conv_output: bfloat16 [65536, 1024], P(('fs', 'tp')), may hold values from -6 to 6
- block_cotangent: bfloat16 [65536, 2048], P(('fs', 'tp')), may hold values from -0.09375 to 0.09375
- projectors: bfloat16 [2048, 2, 256], P('fs'), may hold values from -0.125 to 0.125
- first_moment: float32 [256, 2, 1024], P('fs', None, 'tp'), may hold values from -6 to 6
- second_moment: float32 [256, 2, 1024], P('fs', None, 'tp'), may hold values from 0.25 to 4
- gate_master: float32 [2048, 1024], P('fs', 'tp'), may hold values from -0.125 to 0.125
- out_master: float32 [1024, 2048], P('tp', 'fs'), may hold values from -0.1875 to 0.1875
Outputs:
- first_new: float32 [256, 2, 1024], P('fs', None, 'tp')
- second_new: float32 [256, 2, 1024], P('fs', None, 'tp')
- step_gate: float32 [2048, 1024], P('fs', 'tp')
- step_out: float32 [1024, 2048], P('tp', 'fs')
- gate_new: float32 [2048, 1024], P('fs', 'tp')
- out_new: float32 [1024, 2048], P('tp', 'fs')
- gate_copy: bfloat16 [2048, 1024], P(None, 'tp')
- out_copy: bfloat16 [1024, 2048], P('tp')
All inputs are finite; a program needn't handle non-finite values.
Results may differ from a plain program's by a relative error of at most 0.0035.
Values may be sent and summed in bfloat16 or wider, within the bound.
A program may use at most 64 MiB of HBM per device.

v0:
```python
import math

import jax
import jax.numpy as jnp
from jax import lax
from jax.sharding import Mesh
from jax.sharding import PartitionSpec as P

CH = 1024
RANK = 256
TP = ("tp_0", "tp_1")
FS = ("fs_0", "fs_1")
FS_TP = ("fs_0", "fs_1", "tp_0", "tp_1")


BETA_FIRST = 0.8
BETA_SECOND = 0.9
LEARN_RATE = 0.01
CLIP_SHARE = 0.5
HIGHEST_MODE = lax.Precision.HIGHEST


def joined_along(parts, dim):
    parts = jnp.moveaxis(parts, 0, dim)
    dims = parts.shape
    return parts.reshape(*dims[:dim], dims[dim] * dims[dim + 1], *dims[dim + 2 :])


def copy_for_each(shard, axis):
    count = lax.axis_size(axis)
    return lax.all_to_all(
        jnp.broadcast_to(shard[None], (count, *shard.shape)), axis, 0, 0, tiled=True
    )


def gathered_copies(shard, axis, dim):
    return joined_along(copy_for_each(shard, axis), dim)


def one_axis_at_a_time(shard, axes):
    for axis in axes:
        shard = lax.psum(shard, axis)
    return shard


def turned_gather(arrays, axis, dims):
    turned = [jnp.moveaxis(a, dim, 0) for a, dim in zip(arrays, dims)]
    both = jnp.concatenate([t.reshape(len(t), -1) for t in turned], axis=1)
    out, at, finished = (lax.all_gather(both, axis, axis=0, tiled=True), 0, [])
    for t, dim in zip(turned, dims):
        slab = out[:, at : at + t[0].size].reshape(-1, *t.shape[1:])
        finished.append(jnp.moveaxis(slab, 0, dim))
        at += t[0].size
    return tuple(finished)


def tiled_rows(row_start, row_count, inner_rows, tile_total, builder):
    tile_span = inner_rows * tile_total
    shaped = builder(row_start // tile_span, row_count // tile_span, 0, tile_total)
    return shaped.reshape(row_count, 2, shaped.shape[-1])


def tile_product(left_rows, right_cols, tile_count, width_cols):
    right_part = right_cols
    right_part = right_part.reshape(right_part.shape[0], tile_count, width_cols)
    return jnp.einsum("raq,rtc->atqc", left_rows, right_part, preferred_element_type=jnp.float32)


def split_product(mixed_rows, right_cols, tile_count, width_cols):
    upper_part = lax.optimization_barrier(mixed_rows.astype(jnp.bfloat16))
    lower_part = (mixed_rows - upper_part.astype(jnp.float32)).astype(jnp.bfloat16)
    return tile_product(upper_part, right_cols, tile_count, width_cols) + tile_product(
        lower_part, right_cols, tile_count, width_cols
    )


def shards(
    tokens_in,
    gate_cotangent,
    conv_output,
    block_cotangent,
    projectors,
    first_moment,
    second_moment,
    gate_master,
    out_master,
):
    tile_total = lax.axis_size(TP)
    local_rows = tokens_in.shape[0]
    width_cols = gate_master.shape[1]
    rank_rows = first_moment.shape[0]
    own_proj = projectors.astype(jnp.float32)
    whole_proj = gathered_copies(projectors, FS, 0)

    def low_blocks(first_block, block_count, first_tile, tile_count):
        gate_mix = jnp.dot(tokens_in, whole_proj[:, 0, :], preferred_element_type=jnp.float32)
        flip_mix = jnp.dot(block_cotangent, whole_proj[:, 1, :], preferred_element_type=jnp.float32)
        gate_mix = gate_mix.reshape(local_rows, block_count, rank_rows)
        flip_mix = flip_mix.reshape(local_rows, block_count, rank_rows)
        gate_term = split_product(gate_mix, gate_cotangent, tile_count, width_cols)
        flip_term = split_product(flip_mix, conv_output, tile_count, width_cols)
        return jnp.stack((gate_term, flip_term), axis=3)

    low_space = lax.psum_scatter(
        tiled_rows(
            jnp.int32(0), rank_rows * lax.axis_size(FS_TP), rank_rows, tile_total, low_blocks
        ),
        FS_TP,
        scatter_dimension=0,
        tiled=True,
    )
    first_new = BETA_FIRST * first_moment + (1.0 - BETA_FIRST) * low_space
    second_new = BETA_SECOND * second_moment + (1.0 - BETA_SECOND) * low_space * low_space
    direction = first_new / jnp.sqrt(second_new)
    squares = jnp.sum(direction * direction, axis=(0, 2))
    global_sums = one_axis_at_a_time(squares, FS_TP)
    clip_level = CLIP_SHARE * math.sqrt(RANK * CH)
    factor = clip_level / jnp.maximum(jnp.sqrt(global_sums), clip_level)
    raw_step = jnp.einsum(
        "dmr,rmc->dmc", own_proj, gathered_copies(direction, FS, 0), precision=HIGHEST_MODE
    )
    scaled_step = raw_step * factor[None, :, None]
    step_gate = scaled_step[:, 0, :]
    step_out = scaled_step[:, 1, :].T
    gate_new = gate_master - LEARN_RATE * step_gate
    out_new = out_master - LEARN_RATE * step_out
    gate_copy, out_copy = turned_gather(
        (gate_new.astype(jnp.bfloat16), out_new.astype(jnp.bfloat16)), FS, (0, 1)
    )
    return (first_new, second_new, step_gate, step_out, gate_new, out_new, gate_copy, out_copy)


def solution(mesh):
    split = Mesh(mesh.devices.reshape(4, 4, 8, 2), ("fs_0", "fs_1", "tp_0", "tp_1"))
    in_specs = (
        P(FS_TP, None),
        P(FS_TP, None),
        P(FS_TP, None),
        P(FS_TP, None),
        P(FS, None, None),
        P(FS, None, TP),
        P(FS, None, TP),
        P(FS, TP),
        P(TP, FS),
    )
    out_specs = (
        P(FS, None, TP),
        P(FS, None, TP),
        P(FS, TP),
        P(TP, FS),
        P(FS, TP),
        P(TP, FS),
        P(None, TP),
        P(TP, None),
    )
    return jax.shard_map(
        shards, mesh=split, in_specs=in_specs, out_specs=out_specs, check_vma=False
    )
```

profile of v0, /device:TPU:1, one launch (start us, length us, event | category | flops | bytes accessed | tf_op | source)
XLA Modules:
  0.0 412.0 jit_solution(17500356495709427606)
XLA Ops:
  7.2 1.1 copy.43
  8.3 1.8 broadcast_in_dim.4
  10.1 7.6 %all-to-all-start = ((bf16[16,128,2,256]{1,3,2,0:T(8,128)(2,1)}), bf16[16,128,2,256]{1,3,2,0:T(8,128)(2,1)S(1)}, u32[]{:S(2)}, u32[]{:S(2)}) async-start(bf16[16,128,2,256]{1,3,2,0:T(8,128)(2,1)} %broadcast_in_dim.4), calls=%async_computation | async-start | bytes 4194304 | tf_op jit(solution)/shard_map/all_to_all | solution.py:31
  17.8 2.1 copy.46
  19.8 2.0 copy.48
  21.9 26.8 %all-to-all-done = bf16[16,128,2,256]{1,3,2,0:T(8,128)(2,1)S(1)} async-done(((bf16[16,128,2,256]{1,3,2,0:T(8,128)(2,1)}), bf16[16,128,2,256]{1,3,2,0:T(8,128)(2,1)S(1)}, u32[]{:S(2)}, u32[]{:S(2)}) %all-to-all-start) | async-done | bytes 2097184 | tf_op jit(solution)/shard_map/all_to_all | solution.py:31
  48.7 2.6 copy.44
  51.3 1.7 slice_bitcast_fusion.1
  53.0 1.4 copy.45
  54.4 1.7 fusion.17
  56.1 1.4 copy.47
  57.6 2.0 fusion.16
  62.0 5.7 %pad_maximum_fusion = f32[4096,2,64]{2,1,0:T(2,128)} fusion(f32[4096,1,64]{2,1,0:T(1,128)S(1)} %bitcast.85, f32[4096,1,64]{2,1,0:T(1,128)S(1)} %bitcast.84), kind=kLoop, calls=%fused_computation | loop fusion | flops 524288 | bytes 4194304 | tf_op jit(solution)/shard_map/stack | solution.py:102
  67.8 269.0 %all-reduce.3.cloned.1.call-done = f32[4096,2,64]{2,1,0:T(2,128)} async-done(((f32[4096,2,64]{2,1,0:T(2,128)}), f32[4096,2,64]{2,1,0:T(2,128)}) %all-reduce.3.cloned.1.call-update) | async-done | bytes 2097168
  336.8 1.5 multiply_reduce_fusion
  338.3 8.4 %psum.28 = f32[2]{0:T(128)S(1)} all-reduce(f32[2]{0:T(128)S(1)} %get-tuple-element.14), channel_id=1, replica_groups=mesh['fs_0'=4,'fs_1'=4,'tp_0'=8,'tp_1'=2] {'fs_0'}, use_global_device_ids=true, to_apply=%region_2.0 | all-reduce | flops 2 | bytes 16 | tf_op jit(solution)/shard_map/psum | solution.py:42
  346.8 8.4 %psum.29 = f32[2]{0:T(128)S(1)} all-reduce(f32[2]{0:T(128)S(1)} %psum.28), channel_id=1, replica_groups=mesh['fs_0'=4,'fs_1'=4,'tp_0'=8,'tp_1'=2] {'fs_1'}, use_global_device_ids=true, to_apply=%region_3.0 | all-reduce | flops 2 | bytes 16 | tf_op jit(solution)/shard_map/psum | solution.py:42
  355.1 0.8 reshape.54
  356.0 14.0 %psum.30 = f32[2]{0:T(128)S(1)} all-reduce(f32[2]{0:T(128)S(1)} %psum.29), channel_id=1, replica_groups=mesh['fs_0'=4,'fs_1'=4,'tp_0'=8,'tp_1'=2] {'tp_0'}, use_global_device_ids=true, to_apply=%region_4.0 | all-reduce | flops 2 | bytes 16 | tf_op jit(solution)/shard_map/psum | solution.py:42
  369.9 3.5 all-to-all-start.1
  373.5 7.9 %psum.31 = f32[2]{0:T(128)S(1)} all-reduce(f32[2]{0:T(128)S(1)} %psum.30), channel_id=1, replica_groups=mesh['fs_0'=4,'fs_1'=4,'tp_0'=8,'tp_1'=2] {'tp_1'}, use_global_device_ids=true, to_apply=%region_5.0 | all-reduce | flops 2 | bytes 16 | tf_op jit(solution)/shard_map/psum | solution.py:42
  381.9 0.9 reduce
  384.6 19.7 %all_gather.3 = bf16[2048,128]{0,1:T(8,128)(2,1)S(1)} all-gather(bf16[128,128]{0,1:T(8,128)(2,1)S(1)} %pad_maximum_fusion.1), channel_id=1, replica_groups=mesh['fs_0'=4,'fs_1'=4,'tp_0'=8,'tp_1'=2] {'fs_0','fs_1'}, dimensions={0}, use_global_device_ids=true | all-gather | bytes 557056 | tf_op jit(solution)/shard_map/all_gather | solution.py:49
  404.4 0.8 slice_bitcast_fusion.2
  (31 shorter events, 4.8 us)
Async XLA Ops:
  7.2 47.2 %copy-start = (bf16[256,2048]{1,0:T(8,128)(2,1)S(1)}, bf16[256,2048]{1,0:T(8,128)(2,1)}, u32[]{:S(2)}) copy-start(bf16[256,2048]{1,0:T(8,128)(2,1)} %param.9) | copy-start | bytes 3145732
  10.1 38.5 %all-to-all-start = ((bf16[16,128,2,256]{1,3,2,0:T(8,128)(2,1)}), bf16[16,128,2,256]{1,3,2,0:T(8,128)(2,1)S(1)}, u32[]{:S(2)}, u32[]{:S(2)}) async-start(bf16[16,128,2,256]{1,3,2,0:T(8,128)(2,1)} %broadcast_in_dim.4), calls=%async_computation | async-start | bytes 4194304 | tf_op jit(solution)/shard_map/all_to_all | solution.py:31
  17.7 319.1 %all-reduce.3.cloned.1.call-start = ((), (), s32[]{:S(2)}) async-start(), calls=%async_computation.2 | async-start | bytes 8388608
  56.1 3.5 copy-start.2
  60.0 1.0 copy-start.1
  67.7 269.1 %copy-start.5 = (f32[16,2,64]{2,1,0:T(2,128)S(1)}, f32[16,2,64]{2,1,0:T(2,128)}, u32[]{:S(2)}) copy-start(f32[16,2,64]{2,1,0:T(2,128)} %param.15) | copy-start | bytes 24580
  67.7 269.1 %copy-start.6 = (f32[16,2,64]{2,1,0:T(2,128)S(1)}, f32[16,2,64]{2,1,0:T(2,128)}, u32[]{:S(2)}) copy-start(f32[16,2,64]{2,1,0:T(2,128)} %param.14) | copy-start | bytes 24580
  67.8 315.6 %copy-start.3 = (f32[64,128]{1,0:T(8,128)S(1)}, f32[64,128]{1,0:T(8,128)}, u32[]{:S(2)}) copy-start(f32[64,128]{1,0:T(8,128)} %param.17) | copy-start | bytes 98308
  67.8 316.2 %copy-start.4 = (f32[128,64]{0,1:T(8,128)S(1)}, f32[128,64]{0,1:T(8,128)}, u32[]{:S(2)}) copy-start(f32[128,64]{0,1:T(8,128)} %param.16) | copy-start | bytes 98308
  369.9 11.4 %all-to-all-start.1 = ((f32[16,1,2048]{2,1,0:T(1,128)}), f32[16,1,2048]{2,1,0:T(1,128)S(1)}, u32[]{:S(2)}, u32[]{:S(2)}) async-start(f32[16,1,2048]{2,1,0:T(1,128)} %reshape.54), calls=%async_computation.1 | async-start | bytes 262144 | tf_op jit(solution)/shard_map/all_to_all | solution.py:31
Sparse Core Ops, SparseCore 0:
  67.9 268.9 all-reduce.2
where the time goes:
time: 419 us; the launch traced here: 412 us
  waiting for transfers between devices  296 us (71%)
  blocking collectives  58.4 us (14%)
  local copies, waits for them, and re-layouts  17.1 us (4%)
  between operations  14.2 us (3%)
  starting transfers between devices  11.1 us (3%)
  other arithmetic  9.44 us (2%)
  matrix products  5.9 us (1%)
    unnamed x2, waiting for transfers between devices  269 us
    psum x4, blocking collectives, one_axis_at_a_time(): shard = lax.psum(shard, axis)  38.6 us
    all_to_all x2, waiting for transfers between devices, copy_for_each(): lax.all_to_all(jnp.broadcast_to(shard[None], (count, *shard.shape)), axis...  26.8 us
    all_gather x1, blocking collectives, turned_gather(): out, at, finished = (lax.all_gather(both, axis, axis=0, tiled=True), 0, [])  19.7 us
    all_to_all x2, starting transfers between devices, copy_for_each(): lax.all_to_all(jnp.broadcast_to(shard[None], (count, *shard.shape)), axis...  11.1 us
  transfers between devices with their start and end apart: 3, of which 2 were waited for; matrix products, arithmetic and copies ran while one was open for 1% of the time, Pallas kernels for 0%

commit v1 on v0

v1 whole, which is shorter than its diff:
```python
import functools
import math

import jax
import jax.numpy as jnp
from jax import lax
from jax.experimental import pallas as pl
from jax.experimental.pallas import tpu as pltpu
from jax.sharding import Mesh
from jax.sharding import PartitionSpec as P

MESH = pl.DeviceIdType.MESH
F32 = jnp.float32
BF16 = jnp.bfloat16
FS = ("y", "x")
TP = ("z", "c")
FS_TP = ("y", "x", "z", "c")

BETA_FIRST = 0.8
BETA_SECOND = 0.9
LEARN_RATE = 0.01
CLIP_SHARE = 0.5


def kernel(
    sizes,
    x_hbm,
    g_hbm,
    cv_hbm,
    b_hbm,
    proj,
    fm,
    sm,
    gm,
    om,
    fn_out,
    sn_out,
    sg_out,
    so_out,
    gn_out,
    on_out,
    gc_out,
    oc_out,
    ax,
    ag,
    pfull,
    mix,
    low,
    lowb,
    rs,
    psf,
    psb,
    zb,
    dall,
    cb,
    ebuf,
    load_sem,
    swap_send,
    swap_recv,
    pf_send,
    pf_recv,
    pa_send,
    pa_recv,
    pb_send,
    pb_recv,
    rs_send,
    rs_recv,
    z_send,
    z_recv,
    d_send,
    d_recv,
    c_send,
    c_recv,
    e_send,
    e_recv,
):
    NY, NX, NZ = sizes
    NFS = NY * NX
    tokens = x_hbm.shape[0]
    rows = proj.shape[0]
    rank = pfull.shape[1]
    rk = rank // NFS
    width = zb.shape[-1]
    half = width // 2
    y, x = lax.axis_index("y"), lax.axis_index("x")
    z, c = lax.axis_index("z"), lax.axis_index("c")
    fs = y * NX + x

    def fs_peer(d):
        return (lax.rem(y + d // NX, NY), lax.rem(x + d % NX, NX), z, c)

    def fs_source(d):
        return lax.rem(y + NY - d // NX, NY) * NX + lax.rem(x + NX - d % NX, NX)

    def tp_peer(e):
        return (y, x, lax.rem(z + e // 2, NZ), lax.rem(c + e % 2, 2))

    partner = (y, x, z, 1 - c)

    def own_loads(act, cot):
        return (
            pltpu.make_async_copy(act, ax.at[0], load_sem.at[0]),
            pltpu.make_async_copy(cot, ag.at[0], load_sem.at[1]),
        )

    def swaps(act, cot):
        return (
            pltpu.make_async_remote_copy(
                act, ax.at[1], swap_send.at[0], swap_recv.at[0], device_id=partner, device_id_type=MESH
            ),
            pltpu.make_async_remote_copy(
                cot, ag.at[1], swap_send.at[1], swap_recv.at[1], device_id=partner, device_id_type=MESH
            ),
        )

    @pl.when(c == 0)
    def _():
        for copy in own_loads(x_hbm, g_hbm):
            copy.start()

    @pl.when(c == 1)
    def _():
        for copy in own_loads(b_hbm, cv_hbm):
            copy.start()

    barrier = pltpu.get_barrier_semaphore()

    @pl.loop(1, NFS)
    def _(d):
        pl.semaphore_signal(barrier, inc=1, device_id=fs_peer(d), device_id_type=MESH)

    @pl.loop(1, 2 * NZ)
    def _(e):
        pl.semaphore_signal(barrier, inc=1, device_id=tp_peer(e), device_id_type=MESH)

    own = pl.multiple_of(fs * rows, rows)
    slab = proj[...]
    pfull[pl.ds(own, rows), :] = jnp.where(c == 0, slab[:, 0, :], slab[:, 1, :])
    pl.semaphore_wait(barrier, NFS - 1 + 2 * NZ - 1)

    def p_copy(src, first, count, send, recv, d, peer):
        at = pl.ds(pl.multiple_of(src * rows + first, count), count)
        return pltpu.make_async_remote_copy(
            pfull.at[at], pfull.at[at], send.at[d], recv.at[d], device_id=peer, device_id_type=MESH
        )

    hr = rows // 2
    axis_offsets = [k for k in range(1, NX)] + [k * NX for k in range(1, NY)]
    for d in axis_offsets:
        p_copy(fs, 0, rows, pf_send, pf_recv, d, fs_peer(d)).start()

    @pl.when(c == 0)
    def _():
        for copy in swaps(b_hbm, cv_hbm):
            copy.start()

    @pl.when(c == 1)
    def _():
        for copy in swaps(x_hbm, g_hbm):
            copy.start()

    for k in range(1, max(NX, NY)):
        if k < NX:
            p_copy(fs_source(k), 0, rows, pf_send, pf_recv, k, fs_peer(k)).wait_recv()
            for j in range(1, NY):
                p_copy(fs_source(k), 0, hr, pa_send, pa_recv, j * NX + k, fs_peer(j * NX)).start()
        if k < NY:
            p_copy(fs_source(k * NX), 0, rows, pf_send, pf_recv, k * NX, fs_peer(k * NX)).wait_recv()
            for j in range(1, NX):
                p_copy(fs_source(k * NX), hr, hr, pb_send, pb_recv, k * NX + j, fs_peer(j)).start()

    for copy in own_loads(x_hbm, g_hbm):
        copy.wait()
    for copy in swaps(x_hbm, g_hbm):
        copy.wait_recv()

    for dy in range(NY):
        if dy > 0:
            for dx in range(1, NX):
                d = dy * NX + dx
                p_copy(fs_source(d), 0, hr, pa_send, pa_recv, d, fs_peer(d)).wait_recv()
                p_copy(fs_source(d), hr, hr, pb_send, pb_recv, d, fs_peer(d)).wait_recv()
        ydim = lax.rem(y + NY - dy, NY)
        at = pl.ds(pl.multiple_of(ydim * (NX * rows), NX * rows), NX * rows)
        for s in range(2):
            term = jnp.dot(ax[s, :, at], pfull[at, :], preferred_element_type=F32)
            span = pl.ds(s * tokens, tokens)
            if dy == 0:
                mix[span, :] = term
            else:
                mix[span, :] += term

    both = mix[...]
    upper = both.astype(BF16)
    lower = (both - upper.astype(F32)).astype(BF16)
    cots = ag[...].reshape(2 * tokens, ag.shape[-1])
    turn = (((0,), (0,)), ((), ()))
    low[...] = lax.dot_general(upper, cots, turn, preferred_element_type=F32) + lax.dot_general(
        lower, cots, turn, preferred_element_type=F32
    )
    lowb[...] = low[...].astype(BF16)

    def rs_copy(d, dst):
        return pltpu.make_async_remote_copy(
            lowb.at[pl.ds(pl.multiple_of(dst * rk, rk), rk)],
            rs.at[d],
            rs_send.at[d],
            rs_recv.at[d],
            device_id=fs_peer(d),
            device_id_type=MESH,
        )

    def fs_target(d):
        return lax.rem(y + d // NX, NY) * NX + lax.rem(x + d % NX, NX)

    for d in range(1, NFS):
        rs_copy(d, fs_target(d)).start()
    total = low[pl.ds(pl.multiple_of(fs * rk, rk), rk), :]
    for d in range(1, NFS):
        rs_copy(d, fs).wait_recv()
        total = total + rs[d].astype(F32)
    psf[...] = total
    psb[...] = total.astype(BF16)

    def z_copy(e):
        zt = lax.rem(z + e // 2, NZ)
        return pltpu.make_async_remote_copy(
            psb.at[:, pl.ds(pl.multiple_of(zt * width, width), width)],
            zb.at[e],
            z_send.at[e],
            z_recv.at[e],
            device_id=tp_peer(e),
            device_id_type=MESH,
        )

    for e in range(1, 2 * NZ):
        z_copy(e).start()
    same = psf[:, pl.ds(pl.multiple_of(z * width, width), width)]
    other = jnp.zeros_like(same)
    for e in range(1, 2 * NZ):
        z_copy(e).wait_recv()
        if e % 2:
            other = other + zb[e].astype(F32)
        else:
            same = same + zb[e].astype(F32)

    fm_in, sm_in = fm[...], sm[...]
    directions = []
    for m in range(2):
        whole = jnp.where(c == m, same, other)
        part = jnp.where(c == 0, whole[:, :half], whole[:, half:])
        first = BETA_FIRST * fm_in[:, m, :] + (1.0 - BETA_FIRST) * part
        second = BETA_SECOND * sm_in[:, m, :] + (1.0 - BETA_SECOND) * part * part
        fn_out[:, m, :] = first
        sn_out[:, m, :] = second
        directions.append(first / jnp.sqrt(second))
    mine = pl.ds(pl.multiple_of(fs * rk, rk), rk)
    dall[mine, :] = jnp.concatenate(directions, axis=1).astype(BF16)

    def d_copy(d, src):
        at = pl.ds(pl.multiple_of(src * rk, rk), rk)
        return pltpu.make_async_remote_copy(
            dall.at[at], dall.at[at], d_send.at[d], d_recv.at[d], device_id=fs_peer(d), device_id_type=MESH
        )

    for d in range(1, NFS):
        d_copy(d, fs).start()
    for d in range(1, NFS):
        d_copy(d, fs_source(d)).wait_recv()

    rotated = dall[...]
    wide = rotated.astype(F32)
    cb[0] = jnp.sum((wide * wide).reshape(rank // 8, 8, width), axis=0)

    def c_copy(e):
        return pltpu.make_async_remote_copy(
            cb.at[0], cb.at[e], c_send.at[e], c_recv.at[e], device_id=tp_peer(e), device_id_type=MESH
        )

    for e in range(1, 2 * NZ):
        c_copy(e).start()

    raws = []
    for m in range(2):
        raw = lax.dot_general(rotated, slab[:, m, :], (((0,), (1,)), ((), ())), preferred_element_type=F32)
        raws.append(raw[m * half : (m + 1) * half])

    squares = cb[0]
    for e in range(1, 2 * NZ):
        c_copy(e).wait_recv()
        squares = squares + cb[e]
    clip_level = CLIP_SHARE * math.sqrt(rank * width * NZ)
    masters = (gm, om)
    steps = (sg_out, so_out)
    news = (gn_out, on_out)
    for m in range(2):
        norm = jnp.sqrt(jnp.sum(squares[:, m * half : (m + 1) * half], axis=(0, 1), keepdims=True))
        factor = clip_level / jnp.maximum(norm, clip_level)
        step = raws[m] * factor
        new = masters[m][...] - LEARN_RATE * step
        steps[m][...] = step
        news[m][...] = new
        ebuf[m, :, pl.ds(own, rows)] = new.astype(BF16)

    def e_copy(d, src):
        at = pl.ds(pl.multiple_of(src * rows, rows), rows)
        return pltpu.make_async_remote_copy(
            ebuf.at[:, :, at], ebuf.at[:, :, at], e_send.at[d], e_recv.at[d], device_id=fs_peer(d), device_id_type=MESH
        )

    for d in range(1, NFS):
        e_copy(d, fs).start()
    for d in range(1, NFS):
        e_copy(d, fs_source(d)).wait_recv()
    gc_out[...] = ebuf[0]
    oc_out[...] = ebuf[1]

    for d in axis_offsets:
        p_copy(fs, 0, rows, pf_send, pf_recv, d, fs_peer(d)).wait_send()
    for d in range(1, NFS):
        if d // NX and d % NX:
            p_copy(fs, 0, hr, pa_send, pa_recv, d, fs_peer(d)).wait_send()
            p_copy(fs, hr, hr, pb_send, pb_recv, d, fs_peer(d)).wait_send()
        rs_copy(d, fs).wait_send()
        d_copy(d, fs).wait_send()
        e_copy(d, fs).wait_send()
    for e in range(1, 2 * NZ):
        z_copy(e).wait_send()
        c_copy(e).wait_send()
    for copy in swaps(x_hbm, g_hbm):
        copy.wait_send()


def shards(sizes, x, g, cv, b, proj, fm, sm, gm, om):
    NY, NX, NZ = sizes
    NFS = NY * NX
    tokens, d_model = x.shape
    channels = g.shape[1]
    rows, _, rank = proj.shape
    rk = rank // NFS
    cols = gm.shape[1]
    width = 2 * cols
    vmem = pl.BlockSpec(memory_space=pltpu.VMEM)
    hbm = pl.BlockSpec(memory_space=pl.ANY)
    dma = pltpu.SemaphoreType.DMA
    small = jax.ShapeDtypeStruct(fm.shape, F32)
    block = jax.ShapeDtypeStruct((cols, rows), F32)
    copy = jax.ShapeDtypeStruct((cols, d_model), BF16)
    fn, sn, sg, so, gn, on, gc, oc = pl.pallas_call(
        functools.partial(kernel, sizes),
        out_shape=(small, small, block, block, block, block, copy, copy),
        in_specs=[hbm] * 4 + [vmem] * 5,
        out_specs=(vmem,) * 8,
        scratch_shapes=[
            pltpu.VMEM((2, tokens, d_model), BF16),
            pltpu.VMEM((2, tokens, channels), BF16),
            pltpu.VMEM((d_model, rank), BF16),
            pltpu.VMEM((2 * tokens, rank), F32),
            pltpu.VMEM((rank, channels), F32),
            pltpu.VMEM((rank, channels), BF16),
            pltpu.VMEM((NFS, rk, channels), BF16),
            pltpu.VMEM((rk, channels), F32),
            pltpu.VMEM((rk, channels), BF16),
            pltpu.VMEM((2 * NZ, rk, width), BF16),
            pltpu.VMEM((rank, width), BF16),
            pltpu.VMEM((2 * NZ, 8, width), F32),
            pltpu.VMEM((2, cols, d_model), BF16),
            dma((2,)),
            dma((2,)),
            dma((2,)),
        ]
        + [dma((NFS,))] * 8
        + [dma((2 * NZ,))] * 2
        + [dma((NFS,))] * 2
        + [dma((2 * NZ,))] * 2
        + [dma((NFS,))] * 2,
        compiler_params=pltpu.CompilerParams(collective_id=0, has_side_effects=True, vmem_limit_bytes=48 * 2**20),
    )(x, g, cv, b, proj, fm, sm, gm.T, om)
    return fn, sn, sg.T, so, gn.T, on, gc.T, oc


def solution(mesh):
    sizes = (4, 4, 8)
    split = Mesh(mesh.devices.reshape(*sizes, 2), FS_TP)
    return build(split, sizes)


def build(split, sizes):
    in_specs = (
        P(FS_TP, None),
        P(FS_TP, None),
        P(FS_TP, None),
        P(FS_TP, None),
        P(FS, None, None),
        P(FS, None, TP),
        P(FS, None, TP),
        P(FS, TP),
        P(TP, FS),
    )
    out_specs = (
        P(FS, None, TP),
        P(FS, None, TP),
        P(FS, TP),
        P(TP, FS),
        P(FS, TP),
        P(TP, FS),
        P(None, TP),
        P(TP, None),
    )
    return jax.shard_map(
        functools.partial(shards, sizes), mesh=split, in_specs=in_specs, out_specs=out_specs, check_vma=False
    )
```

time: 419 us -> 73.1 us (0.17); the launches traced: 412 us -> 72.6 us
  waiting for transfers between devices: 296 us -> 0 us
  Pallas kernels: 0 us -> 58.5 us
  blocking collectives: 58.4 us -> 0 us
  between operations: 14.2 us -> 0.66 us
  starting transfers between devices: 11.1 us -> 0 us
  other arithmetic: 9.44 us -> 0 us
  matrix products: 5.9 us -> 0 us
    unnamed x2 -> x0, waiting for transfers between devices: 269 us -> none
    pallas_call x0 -> x1, Pallas kernels: none -> 58.5 us  [shards(): pl.pallas_call(functools.partial(kernel, sizes), out_shape=(small, small,...]
    psum x4 -> x0, blocking collectives: 38.6 us -> none  [one_axis_at_a_time(): shard = lax.psum(shard, axis)]
    all_to_all x2 -> x0, waiting for transfers between devices: 26.8 us -> none  [copy_for_each(): lax.all_to_all(jnp.broadcast_to(shard[None], (count, *shard.shape)), axis...]
    all_gather x1 -> x0, blocking collectives: 19.7 us -> none  [turned_gather(): out, at, finished = (lax.all_gather(both, axis, axis=0, tiled=True), 0, [])]
    all_to_all x2 -> x0, starting transfers between devices: 11.1 us -> none  [copy_for_each(): lax.all_to_all(jnp.broadcast_to(shard[None], (count, *shard.shape)), axis...]
    unnamed x20 -> x26, local copies, waits for them, and re-layouts: 6.79 us -> 13.5 us
    dot_general x7 -> x0, matrix products: 5.9 us -> none  [the longest x1 2.01 us: low_blocks(): jnp.dot(block_cotangent, whole_proj[:, 1, :], preferred_element_type=jnp....]
  transfers between devices with their start and end apart: 3 -> 0, of which waited for: 2 -> 0; matrix products, arithmetic and copies ran while one was open for 1% -> 0% of each run, Pallas kernels for 0% -> 0%
where the time goes in v1:
time: 73.1 us; the launch traced here: 72.6 us
  Pallas kernels  58.5 us (80%)
  local copies, waits for them, and re-layouts  13.5 us (18%)
    pallas_call x1, Pallas kernels, shards(): pl.pallas_call(functools.partial(kernel, sizes), out_shape=(small, small,...  58.5 us
    unnamed x26, local copies, waits for them, and re-layouts  13.5 us

profile of v1, /device:TPU:1, one launch (start us, length us, event | category | flops | bytes accessed | tf_op | source)
XLA Modules:
  0.0 72.6 jit_solution(3615323547359833885)
XLA Ops:
  0.6 0.0 copy-start
  0.6 1.2 %copy-done = bf16[256,2048]{1,0:T(8,128)(2,1)S(1)} copy-done((bf16[256,2048]{1,0:T(8,128)(2,1)S(1)}, bf16[256,2048]{1,0:T(8,128)(2,1)}, u32[]{:S(2)}) %copy-start) | copy-done | bytes 1048600
  1.9 0.0 copy-start.1
  1.9 1.2 %copy-done.1 = bf16[256,2048]{1,0:T(8,128)(2,1)S(1)} copy-done((bf16[256,2048]{1,0:T(8,128)(2,1)S(1)}, bf16[256,2048]{1,0:T(8,128)(2,1)}, u32[]{:S(2)}) %copy-start.1) | copy-done | bytes 1048600
  3.1 0.0 copy-start.2
  3.1 1.0 %copy-done.2 = bf16[256,1024]{1,0:T(8,128)(2,1)S(1)} copy-done((bf16[256,1024]{1,0:T(8,128)(2,1)S(1)}, bf16[256,1024]{1,0:T(8,128)(2,1)}, u32[]{:S(2)}) %copy-start.2) | copy-done | bytes 524312
  4.1 0.0 copy-start.3
  4.1 1.0 %copy-done.3 = bf16[256,1024]{1,0:T(8,128)(2,1)S(1)} copy-done((bf16[256,1024]{1,0:T(8,128)(2,1)S(1)}, bf16[256,1024]{1,0:T(8,128)(2,1)}, u32[]{:S(2)}) %copy-start.3) | copy-done | bytes 524312
  5.2 0.0 copy-start.4
  5.2 0.9 %copy-done.4 = bf16[128,2,256]{2,1,0:T(2,128)(2,1)S(1)} copy-done((bf16[128,2,256]{2,1,0:T(2,128)(2,1)S(1)}, bf16[128,2,256]{2,1,0:T(2,128)(2,1)}, u32[]{:S(2)}) %copy-start.4) | copy-done | bytes 131096
  6.1 0.0 copy-start.5
  6.1 0.8 %copy-done.5 = f32[128,64]{0,1:T(8,128)S(1)} copy-done((f32[128,64]{0,1:T(8,128)S(1)}, f32[128,64]{0,1:T(8,128)}, u32[]{:S(2)}) %copy-start.5) | copy-done | bytes 32792
  6.8 0.8 %copy-done.6 = f32[64,128]{1,0:T(8,128)S(1)} copy-done((f32[64,128]{1,0:T(8,128)S(1)}, f32[64,128]{1,0:T(8,128)}, u32[]{:S(2)}) %copy-start.6) | copy-done | bytes 32792
  7.6 0.7 copy-done.7
  8.3 0.7 copy-done.8
  9.0 58.5 %shard_map.152 = (f32[16,2,64]{2,1,0:T(2,128)S(1)}, f32[16,2,64]{2,1,0:T(2,128)S(1)}, f32[64,128]{1,0:T(8,128)S(1)}, f32[64,128]{1,0:T(8,128)S(1)}, f32[64,128]{...) custom-call(bf16[256,2048]{1,0:T(8,128)(2,1)S(1)} %copy-done, ...), custom_call_target="tpu_custom_call" | custom-call | tf_op jit(solution)/shard_map/pallas_call | solution.py:349
  67.5 0.6 copy.25
  68.1 0.6 copy.26
  68.7 0.6 copy.27
  69.3 0.6 copy.28
  69.9 0.6 copy.29
  70.6 0.6 copy.30
  71.2 0.7 copy.31
  71.9 0.7 copy.32
  (3 shorter events, 0.0 us)
Async XLA Ops:
  0.6 1.2 %copy-start = (bf16[256,2048]{1,0:T(8,128)(2,1)S(1)}, bf16[256,2048]{1,0:T(8,128)(2,1)}, u32[]{:S(2)}) copy-start(bf16[256,2048]{1,0:T(8,128)(2,1)} %x_hbm.1) | copy-start | bytes 3145732
  1.9 1.2 %copy-start.1 = (bf16[256,2048]{1,0:T(8,128)(2,1)S(1)}, bf16[256,2048]{1,0:T(8,128)(2,1)}, u32[]{:S(2)}) copy-start(bf16[256,2048]{1,0:T(8,128)(2,1)} %b_hbm.1) | copy-start | bytes 3145732
  3.1 1.0 %copy-start.2 = (bf16[256,1024]{1,0:T(8,128)(2,1)S(1)}, bf16[256,1024]{1,0:T(8,128)(2,1)}, u32[]{:S(2)}) copy-start(bf16[256,1024]{1,0:T(8,128)(2,1)} %g_hbm.1) | copy-start | bytes 1572868
  4.1 1.0 %copy-start.3 = (bf16[256,1024]{1,0:T(8,128)(2,1)S(1)}, bf16[256,1024]{1,0:T(8,128)(2,1)}, u32[]{:S(2)}) copy-start(bf16[256,1024]{1,0:T(8,128)(2,1)} %cv_hbm.1) | copy-start | bytes 1572868
  5.2 0.9 %copy-start.4 = (bf16[128,2,256]{2,1,0:T(2,128)(2,1)S(1)}, bf16[128,2,256]{2,1,0:T(2,128)(2,1)}, u32[]{:S(2)}) copy-start(bf16[128,2,256]{2,1,0:T(2,128)(2,1)} %proj.1) | copy-start | bytes 393220
  6.1 0.8 %copy-start.5 = (f32[128,64]{0,1:T(8,128)S(1)}, f32[128,64]{0,1:T(8,128)}, u32[]{:S(2)}) copy-start(f32[128,64]{0,1:T(8,128)} %param.16) | copy-start | bytes 98308
  6.8 0.8 %copy-start.6 = (f32[64,128]{1,0:T(8,128)S(1)}, f32[64,128]{1,0:T(8,128)}, u32[]{:S(2)}) copy-start(f32[64,128]{1,0:T(8,128)} %om.1) | copy-start | bytes 98308
  7.6 0.7 copy-start.7
  8.3 0.7 copy-start.8

commit v2 on v1

--- a/solution.py
+++ b/solution.py
@@ -28,22 +28,26 @@
     g_hbm,
     cv_hbm,
     b_hbm,
-    proj,
-    fm,
-    sm,
-    gm,
-    om,
+    proj_hbm,
+    fm_hbm,
+    sm_hbm,
+    gm_hbm,
+    om_hbm,
     fn_out,
     sn_out,
     sg_out,
     so_out,
     gn_out,
     on_out,
-    gc_out,
-    oc_out,
+    ebuf,
+    proj,
+    fm,
+    sm,
     ax,
     ag,
-    pfull,
+    pboth,
+    masters,
+    raws,
     mix,
     low,
     lowb,
@@ -53,7 +57,6 @@
     zb,
     dall,
     cb,
-    ebuf,
     load_sem,
     swap_send,
     swap_recv,
@@ -71,20 +74,26 @@
     d_recv,
     c_send,
     c_recv,
-    e_send,
-    e_recv,
+    po_sem,
+    mf_send,
+    mf_recv,
+    md_send,
+    md_recv,
 ):
     NY, NX, NZ = sizes
     NFS = NY * NX
     tokens = x_hbm.shape[0]
     rows = proj.shape[0]
-    rank = pfull.shape[1]
+    rank = pboth.shape[2]
     rk = rank // NFS
     width = zb.shape[-1]
     half = width // 2
     y, x = lax.axis_index("y"), lax.axis_index("x")
     z, c = lax.axis_index("z"), lax.axis_index("c")
     fs = y * NX + x
+    pfull = pboth.at[c]
+    own = pl.multiple_of(fs * rows, rows)
+    own_lanes = pl.ds(own, rows)
 
     def fs_peer(d):
         return (lax.rem(y + d // NX, NY), lax.rem(x + d % NX, NX), z, c)
@@ -113,6 +122,9 @@
             ),
         )
 
+    proj_load = pltpu.make_async_copy(proj_hbm, proj, load_sem.at[2])
+    proj_load.start()
+
     @pl.when(c == 0)
     def _():
         for copy in own_loads(x_hbm, g_hbm):
@@ -123,6 +135,15 @@
         for copy in own_loads(b_hbm, cv_hbm):
             copy.start()
 
+    late_loads = [
+        pltpu.make_async_copy(src, dst, load_sem.at[3 + i])
+        for i, (src, dst) in enumerate(
+            ((fm_hbm, fm), (sm_hbm, sm), (gm_hbm, masters.at[0, :, own_lanes]), (om_hbm, masters.at[1, :, own_lanes]))
+        )
+    ]
+    for copy in late_loads:
+        copy.start()
+
     barrier = pltpu.get_barrier_semaphore()
 
     @pl.loop(1, NFS)
@@ -133,7 +154,7 @@
     def _(e):
         pl.semaphore_signal(barrier, inc=1, device_id=tp_peer(e), device_id_type=MESH)
 
-    own = pl.multiple_of(fs * rows, rows)
+    proj_load.wait()
     slab = proj[...]
     pfull[pl.ds(own, rows), :] = jnp.where(c == 0, slab[:, 0, :], slab[:, 1, :])
     pl.semaphore_wait(barrier, NFS - 1 + 2 * NZ - 1)
@@ -200,6 +221,11 @@
     )
     lowb[...] = low[...].astype(BF16)
 
+    po_copy = pltpu.make_async_remote_copy(
+        pfull, pfull, po_sem.at[0], po_sem.at[1], device_id=partner, device_id_type=MESH
+    )
+    po_copy.start()
+
     def rs_copy(d, dst):
         return pltpu.make_async_remote_copy(
             lowb.at[pl.ds(pl.multiple_of(dst * rk, rk), rk)],
@@ -235,6 +261,20 @@
 
     for e in range(1, 2 * NZ):
         z_copy(e).start()
+
+    for copy in late_loads:
+        copy.wait()
+
+    def m_copy(m, src, send, recv, d, peer):
+        at = pl.ds(pl.multiple_of(src * rows, rows), rows)
+        return pltpu.make_async_remote_copy(
+            masters.at[m, :, at], masters.at[m, :, at], send.at[m, d], recv.at[m, d], device_id=peer, device_id_type=MESH
+        )
+
+    for d in axis_offsets:
+        for m in range(2):
+            m_copy(m, fs, mf_send, mf_recv, d, fs_peer(d)).start()
+
     same = psf[:, pl.ds(pl.multiple_of(z * width, width), width)]
     other = jnp.zeros_like(same)
     for e in range(1, 2 * NZ):
@@ -280,55 +320,75 @@
     for e in range(1, 2 * NZ):
         c_copy(e).start()
 
-    raws = []
+    for k in range(1, NX):
+        for m in range(2):
+            m_copy(m, fs_source(k), mf_send, mf_recv, k, fs_peer(k)).wait_recv()
+        for j in range(1, NY):
+            m_copy(0, fs_source(k), md_send, md_recv, j * NX + k, fs_peer(j * NX)).start()
+    for k in range(1, NY):
+        for m in range(2):
+            m_copy(m, fs_source(k * NX), mf_send, mf_recv, k * NX, fs_peer(k * NX)).wait_recv()
+        for j in range(1, NX):
+            m_copy(1, fs_source(k * NX), md_send, md_recv, k * NX + j, fs_peer(j)).start()
+
+    po_copy.wait_recv()
+    turned = rotated.T
     for m in range(2):
-        raw = lax.dot_general(rotated, slab[:, m, :], (((0,), (1,)), ((), ())), preferred_element_type=F32)
-        raws.append(raw[m * half : (m + 1) * half])
+        raws[m] = lax.dot_general(
+            turned[m * half : (m + 1) * half], pboth[m], (((1,), (1,)), ((), ())), preferred_element_type=F32
+        )
 
     squares = cb[0]
     for e in range(1, 2 * NZ):
         c_copy(e).wait_recv()
         squares = squares + cb[e]
     clip_level = CLIP_SHARE * math.sqrt(rank * width * NZ)
-    masters = (gm, om)
+    factors = []
+    for m in range(2):
+        norm = jnp.sqrt(jnp.sum(squares[:, m * half : (m + 1) * half], axis=(0, 1), keepdims=True))
+        factors.append(clip_level / jnp.maximum(norm, clip_level))
     steps = (sg_out, so_out)
     news = (gn_out, on_out)
     for m in range(2):
-        norm = jnp.sqrt(jnp.sum(squares[:, m * half : (m + 1) * half], axis=(0, 1), keepdims=True))
-        factor = clip_level / jnp.maximum(norm, clip_level)
-        step = raws[m] * factor
-        new = masters[m][...] - LEARN_RATE * step
+        step = raws[m, :, own_lanes] * factors[m]
         steps[m][...] = step
-        news[m][...] = new
-        ebuf[m, :, pl.ds(own, rows)] = new.astype(BF16)
-
-    def e_copy(d, src):
-        at = pl.ds(pl.multiple_of(src * rows, rows), rows)
-        return pltpu.make_async_remote_copy(
-            ebuf.at[:, :, at], ebuf.at[:, :, at], e_send.at[d], e_recv.at[d], device_id=fs_peer(d), device_id_type=MESH
-        )
-
-    for d in range(1, NFS):
-        e_copy(d, fs).start()
-    for d in range(1, NFS):
-        e_copy(d, fs_source(d)).wait_recv()
-    gc_out[...] = ebuf[0]
-    oc_out[...] = ebuf[1]
+        news[m][...] = masters[m, :, own_lanes] - LEARN_RATE * step
+    for d in range(1, NFS):
+        if d // NX and d % NX:
+            for m in range(2):
+                m_copy(m, fs_source(d), md_send, md_recv, d, fs_peer(d)).wait_recv()
+    for m in range(2):
+        ebuf[m] = (masters[m] - LEARN_RATE * (raws[m] * factors[m])).astype(BF16)
 
     for d in axis_offsets:
         p_copy(fs, 0, rows, pf_send, pf_recv, d, fs_peer(d)).wait_send()
+        for m in range(2):
+            m_copy(m, fs, mf_send, mf_recv, d, fs_peer(d)).wait_send()
+    po_copy.wait_send()
     for d in range(1, NFS):
         if d // NX and d % NX:
             p_copy(fs, 0, hr, pa_send, pa_recv, d, fs_peer(d)).wait_send()
             p_copy(fs, hr, hr, pb_send, pb_recv, d, fs_peer(d)).wait_send()
+            for m in range(2):
+                m_copy(m, fs, md_send, md_recv, d, fs_peer(d)).wait_send()
         rs_copy(d, fs).wait_send()
         d_copy(d, fs).wait_send()
-        e_copy(d, fs).wait_send()
     for e in range(1, 2 * NZ):
         z_copy(e).wait_send()
         c_copy(e).wait_send()
     for copy in swaps(x_hbm, g_hbm):
         copy.wait_send()
+
+
+def store_kernel(*refs):
+    count = (len(refs) - 2) // 2
+    ins, outs, sem = refs[:count], refs[count:-1], refs[-1]
+    sources = [*ins[:-1], ins[-1].at[0], ins[-1].at[1]]
+    copies = [pltpu.make_async_copy(src, dst, sem.at[i]) for i, (src, dst) in enumerate(zip(sources, outs))]
+    for copy in copies:
+        copy.start()
+    for copy in copies:
+        copy.wait()
 
 
 def shards(sizes, x, g, cv, b, proj, fm, sm, gm, om):
@@ -341,20 +401,25 @@
     cols = gm.shape[1]
     width = 2 * cols
     vmem = pl.BlockSpec(memory_space=pltpu.VMEM)
-    hbm = pl.BlockSpec(memory_space=pl.ANY)
+    hbm = pl.BlockSpec(memory_space=pltpu.HBM)
     dma = pltpu.SemaphoreType.DMA
     small = jax.ShapeDtypeStruct(fm.shape, F32)
     block = jax.ShapeDtypeStruct((cols, rows), F32)
     copy = jax.ShapeDtypeStruct((cols, d_model), BF16)
-    fn, sn, sg, so, gn, on, gc, oc = pl.pallas_call(
+    results = pl.pallas_call(
         functools.partial(kernel, sizes),
-        out_shape=(small, small, block, block, block, block, copy, copy),
-        in_specs=[hbm] * 4 + [vmem] * 5,
-        out_specs=(vmem,) * 8,
+        out_shape=(small, small, block, block, block, block, jax.ShapeDtypeStruct((2, cols, d_model), BF16)),
+        in_specs=[hbm] * 9,
+        out_specs=(vmem,) * 7,
         scratch_shapes=[
+            pltpu.VMEM(proj.shape, BF16),
+            pltpu.VMEM(fm.shape, F32),
+            pltpu.VMEM(sm.shape, F32),
             pltpu.VMEM((2, tokens, d_model), BF16),
             pltpu.VMEM((2, tokens, channels), BF16),
-            pltpu.VMEM((d_model, rank), BF16),
+            pltpu.VMEM((2, d_model, rank), BF16),
+            pltpu.VMEM((2, cols, d_model), F32),
+            pltpu.VMEM((2, cols, d_model), F32),
             pltpu.VMEM((2 * tokens, rank), F32),
             pltpu.VMEM((rank, channels), F32),
             pltpu.VMEM((rank, channels), BF16),
@@ -364,8 +429,7 @@
             pltpu.VMEM((2 * NZ, rk, width), BF16),
             pltpu.VMEM((rank, width), BF16),
             pltpu.VMEM((2 * NZ, 8, width), F32),
-            pltpu.VMEM((2, cols, d_model), BF16),
-            dma((2,)),
+            dma((7,)),
             dma((2,)),
             dma((2,)),
         ]
@@ -373,9 +437,18 @@
         + [dma((2 * NZ,))] * 2
         + [dma((NFS,))] * 2
         + [dma((2 * NZ,))] * 2
-        + [dma((NFS,))] * 2,
+        + [dma((2,))]
+        + [dma((2, NFS))] * 4,
         compiler_params=pltpu.CompilerParams(collective_id=0, has_side_effects=True, vmem_limit_bytes=48 * 2**20),
-    )(x, g, cv, b, proj, fm, sm, gm.T, om)
+    )(*(pltpu.with_memory_space_constraint(a, pltpu.HBM) for a in (x, g, cv, b, proj, fm, sm, gm.T, om)))
+    fn, sn, sg, so, gn, on, gc, oc = pl.pallas_call(
+        store_kernel,
+        out_shape=(small, small, block, block, block, block, copy, copy),
+        in_specs=[vmem] * 7,
+        out_specs=(hbm,) * 8,
+        scratch_shapes=[dma((8,))],
+        compiler_params=pltpu.CompilerParams(vmem_limit_bytes=2**20),
+    )(*results)
     return fn, sn, sg.T, so, gn.T, on, gc.T, oc
 
 

time: 73.1 us -> 52.9 us (0.72)
  local copies, waits for them, and re-layouts: 13.5 us -> 0 us
  Pallas kernels: 58.5 us -> 52.1 us
    unnamed x26 -> x0, local copies, waits for them, and re-layouts: 13.5 us -> none
    pallas_call x1, Pallas kernels: 58.5 us -> 51.2 us  [shards(): pl.pallas_call(functools.partial(kernel, sizes), out_shape=(small, small,...]
    pallas_call x0 -> x1, Pallas kernels: none -> 0.92 us  [shards(): pl.pallas_call(store_kernel, out_shape=(small, small, block, block, block...]
where the time goes in v2:
time: 52.9 us; the launch traced here: 52.8 us
  Pallas kernels  52.1 us (98%)
  between operations  0.64 us (1%)
    pallas_call x1, Pallas kernels, shards(): pl.pallas_call(functools.partial(kernel, sizes), out_shape=(small, small,...  51.2 us

profile of v2, /device:TPU:1, one launch (start us, length us, event | category | flops | bytes accessed | tf_op | source)
XLA Modules:
  0.0 52.8 jit_solution(4023455477361333901)
XLA Ops:
  0.6 51.2 %shard_map.152 = (f32[16,2,64]{2,1,0:T(2,128)S(1)}, f32[16,2,64]{2,1,0:T(2,128)S(1)}, f32[64,128]{1,0:T(8,128)S(1)}, f32[64,128]{1,0:T(8,128)S(1)}, f32[64,128]{...) custom-call(bf16[256,2048]{1,0:T(8,128)(2,1)} %x_hbm.1, bf16[256,1024]{1,0:T(8,128)(2,1)} %g_hbm.1, ...), custom_call_target="tpu_custom_call" | custom-call | tf_op jit(solution)/shard_map/pallas_call | solution.py:409
  51.9 0.9 %shard_map.153 = (f32[16,2,64]{2,1,0:T(2,128)}, f32[16,2,64]{2,1,0:T(2,128)}, f32[64,128]{1,0:T(8,128)}, f32[64,128]{1,0:T(8,128)}, f32[64,128]{1,0:T(8,128)}, /...) custom-call(f32[16,2,64]{2,1,0:T(2,128)S(1)} %get-tuple-element.23.refs_0_, ...), custom_call_target="tpu_custom_call" | custom-call | tf_op jit(solution)/shard_map/pallas_call | solution.py:444

commit v3 on v2

--- a/solution.py
+++ b/solution.py
@@ -79,6 +79,7 @@
     mf_recv,
     md_send,
     md_recv,
+    line_sem,
 ):
     NY, NX, NZ = sizes
     NFS = NY * NX
@@ -124,6 +125,12 @@
 
     proj_load = pltpu.make_async_copy(proj_hbm, proj, load_sem.at[2])
     proj_load.start()
+    axis_offsets = [k for k in range(1, NX)] + [k * NX for k in range(1, NY)]
+    z_neighbours = ((y, x, lax.rem(z + 1, NZ), c), (y, x, lax.rem(z + NZ - 1, NZ), c))
+    greeted = [fs_peer(d) for d in axis_offsets] + [partner, *z_neighbours]
+    barrier = pltpu.get_barrier_semaphore()
+    for peer in greeted:
+        pl.semaphore_signal(barrier, inc=1, device_id=peer, device_id_type=MESH)
 
     @pl.when(c == 0)
     def _():
@@ -144,20 +151,18 @@
     for copy in late_loads:
         copy.start()
 
-    barrier = pltpu.get_barrier_semaphore()
-
-    @pl.loop(1, NFS)
-    def _(d):
-        pl.semaphore_signal(barrier, inc=1, device_id=fs_peer(d), device_id_type=MESH)
-
-    @pl.loop(1, 2 * NZ)
-    def _(e):
-        pl.semaphore_signal(barrier, inc=1, device_id=tp_peer(e), device_id_type=MESH)
+    def line_signal(r):
+        for peer in z_neighbours:
+            pl.semaphore_signal(line_sem.at[r], inc=1, device_id=peer, device_id_type=MESH)
+
+    def line_wait(r):
+        pl.semaphore_wait(line_sem.at[r], 2)
 
     proj_load.wait()
     slab = proj[...]
     pfull[pl.ds(own, rows), :] = jnp.where(c == 0, slab[:, 0, :], slab[:, 1, :])
-    pl.semaphore_wait(barrier, NFS - 1 + 2 * NZ - 1)
+    pl.semaphore_wait(barrier, len(greeted))
+    line_signal(0)
 
     def p_copy(src, first, count, send, recv, d, peer):
         at = pl.ds(pl.multiple_of(src * rows + first, count), count)
@@ -166,7 +171,6 @@
         )
 
     hr = rows // 2
-    axis_offsets = [k for k in range(1, NX)] + [k * NX for k in range(1, NY)]
     for d in axis_offsets:
         p_copy(fs, 0, rows, pf_send, pf_recv, d, fs_peer(d)).start()
 
@@ -189,6 +193,9 @@
             p_copy(fs_source(k * NX), 0, rows, pf_send, pf_recv, k * NX, fs_peer(k * NX)).wait_recv()
             for j in range(1, NX):
                 p_copy(fs_source(k * NX), hr, hr, pb_send, pb_recv, k * NX + j, fs_peer(j)).start()
+
+    line_wait(0)
+    line_signal(1)
 
     for copy in own_loads(x_hbm, g_hbm):
         copy.wait()
@@ -211,6 +218,9 @@
             else:
                 mix[span, :] += term
 
+    line_wait(1)
+    line_signal(2)
+
     both = mix[...]
     upper = both.astype(BF16)
     lower = (both - upper.astype(F32)).astype(BF16)
@@ -241,6 +251,8 @@
 
     for d in range(1, NFS):
         rs_copy(d, fs_target(d)).start()
+    line_wait(2)
+    line_signal(3)
     total = low[pl.ds(pl.multiple_of(fs * rk, rk), rk), :]
     for d in range(1, NFS):
         rs_copy(d, fs).wait_recv()
@@ -259,6 +271,7 @@
             device_id_type=MESH,
         )
 
+    line_wait(3)
     for e in range(1, 2 * NZ):
         z_copy(e).start()
 
@@ -438,7 +451,8 @@
         + [dma((NFS,))] * 2
         + [dma((2 * NZ,))] * 2
         + [dma((2,))]
-        + [dma((2, NFS))] * 4,
+        + [dma((2, NFS))] * 4
+        + [pltpu.SemaphoreType.REGULAR((4,))],
         compiler_params=pltpu.CompilerParams(collective_id=0, has_side_effects=True, vmem_limit_bytes=48 * 2**20),
     )(*(pltpu.with_memory_space_constraint(a, pltpu.HBM) for a in (x, g, cv, b, proj, fm, sm, gm.T, om)))
     fn, sn, sg, so, gn, on, gc, oc = pl.pallas_call(

time: 52.9 us -> 49.6 us (0.938)
  Pallas kernels: 52.1 us -> 48.9 us
    pallas_call x1, Pallas kernels: 51.2 us -> 47.9 us  [shards(): pl.pallas_call(functools.partial(kernel, sizes), out_shape=(small, small,...]
where the time goes in v3:
time: 49.6 us; the launch traced here: 49.5 us
  Pallas kernels  48.9 us (99%)
  between operations  0.64 us (1%)
    pallas_call x1, Pallas kernels, shards(): pl.pallas_call(functools.partial(kernel, sizes), out_shape=(small, small,...  47.9 us

profile of v3, /device:TPU:1, one launch (start us, length us, event | category | flops | bytes accessed | tf_op | source)
XLA Modules:
  0.0 49.5 jit_solution(8166831133609949856)
XLA Ops:
  0.6 47.9 %shard_map.152 = (f32[16,2,64]{2,1,0:T(2,128)S(1)}, f32[16,2,64]{2,1,0:T(2,128)S(1)}, f32[64,128]{1,0:T(8,128)S(1)}, f32[64,128]{1,0:T(8,128)S(1)}, f32[64,128]{...) custom-call(bf16[256,2048]{1,0:T(8,128)(2,1)} %x_hbm.1, bf16[256,1024]{1,0:T(8,128)(2,1)} %g_hbm.1, ...), custom_call_target="tpu_custom_call" | custom-call | tf_op jit(solution)/shard_map/pallas_call | solution.py:422
  48.6 0.9 %shard_map.153 = (f32[16,2,64]{2,1,0:T(2,128)}, f32[16,2,64]{2,1,0:T(2,128)}, f32[64,128]{1,0:T(8,128)}, f32[64,128]{1,0:T(8,128)}, f32[64,128]{1,0:T(8,128)}, /...) custom-call(f32[16,2,64]{2,1,0:T(2,128)S(1)} %get-tuple-element.23.refs_0_, ...), custom_call_target="tpu_custom_call" | custom-call | tf_op jit(solution)/shard_map/pallas_call | solution.py:458

commit v4 on v3

v4 whole, which is shorter than its diff:
```python
import functools
import math

import jax
import jax.numpy as jnp
from jax import lax
from jax.experimental import pallas as pl
from jax.experimental.pallas import tpu as pltpu
from jax.sharding import Mesh
from jax.sharding import PartitionSpec as P

MESH = pl.DeviceIdType.MESH
F32 = jnp.float32
BF16 = jnp.bfloat16
FS = ("y", "x")
TP = ("z", "c")
FS_TP = ("y", "x", "z", "c")

BETA_FIRST = 0.8
BETA_SECOND = 0.9
LEARN_RATE = 0.01
CLIP_SHARE = 0.5


def kernel(
    sizes,
    x_hbm,
    g_hbm,
    cv_hbm,
    b_hbm,
    proj_hbm,
    fm_hbm,
    sm_hbm,
    gm_hbm,
    om_hbm,
    fn_out,
    sn_out,
    sg_out,
    so_out,
    gn_out,
    on_out,
    ebuf,
    proj,
    fm,
    sm,
    ax,
    ag,
    pboth,
    masters,
    raws,
    mix,
    low,
    lowb,
    rs,
    psf,
    psb,
    zb,
    dall,
    cb,
    load_sem,
    swap_send,
    swap_recv,
    p_send,
    pf_recv,
    pd_recv,
    rs_send,
    rs_recv,
    z_send,
    z_recv,
    d_send,
    d_recv,
    c_send,
    c_recv,
    po_sem,
    mf_send,
    mf_recv,
    md_send,
    md_recv,
    line_sem,
):
    NY, NX, NZ = sizes
    NFS = NY * NX
    tokens = x_hbm.shape[0]
    rows = proj.shape[0]
    rank = 2 * pboth.shape[3]
    rk = rank // NFS
    width = zb.shape[-1]
    half = width // 2
    y, x = lax.axis_index("y"), lax.axis_index("x")
    z, c = lax.axis_index("z"), lax.axis_index("c")
    fs = y * NX + x
    pfull = pboth.at[c]
    own = pl.multiple_of(fs * rows, rows)
    own_lanes = pl.ds(own, rows)

    def fs_peer(d):
        return (lax.rem(y + d // NX, NY), lax.rem(x + d % NX, NX), z, c)

    def fs_source(d):
        return lax.rem(y + NY - d // NX, NY) * NX + lax.rem(x + NX - d % NX, NX)

    def tp_peer(e):
        return (y, x, lax.rem(z + e // 2, NZ), lax.rem(c + e % 2, 2))

    partner = (y, x, z, 1 - c)

    def hops(k, n):
        return min(k, n - k)

    fs_offsets = sorted(range(1, NFS), key=lambda d: -hops(d // NX, NY) - hops(d % NX, NX))
    tp_offsets = sorted(range(1, 2 * NZ), key=lambda e: -2 * hops(e // 2, NZ) - e % 2)
    y_offsets = sorted(range(1, NY), key=lambda j: -hops(j, NY))
    x_offsets = sorted(range(1, NX), key=lambda j: -hops(j, NX))

    def own_loads(act, cot):
        return (
            pltpu.make_async_copy(act, ax.at[0], load_sem.at[0]),
            pltpu.make_async_copy(cot, ag.at[0], load_sem.at[1]),
        )

    def swaps(act, cot):
        return (
            pltpu.make_async_remote_copy(
                act, ax.at[1], swap_send.at[0], swap_recv.at[0], device_id=partner, device_id_type=MESH
            ),
            pltpu.make_async_remote_copy(
                cot, ag.at[1], swap_send.at[1], swap_recv.at[1], device_id=partner, device_id_type=MESH
            ),
        )

    proj_load = pltpu.make_async_copy(proj_hbm, proj, load_sem.at[2])
    proj_load.start()
    axis_offsets = [k for k in range(1, NX)] + [k * NX for k in range(1, NY)]
    z_neighbours = ((y, x, lax.rem(z + 1, NZ), c), (y, x, lax.rem(z + NZ - 1, NZ), c))
    greeted = [fs_peer(d) for d in axis_offsets] + [partner, *z_neighbours]
    barrier = pltpu.get_barrier_semaphore()
    for peer in greeted:
        pl.semaphore_signal(barrier, inc=1, device_id=peer, device_id_type=MESH)

    @pl.when(c == 0)
    def _():
        for copy in own_loads(x_hbm, g_hbm):
            copy.start()

    @pl.when(c == 1)
    def _():
        for copy in own_loads(b_hbm, cv_hbm):
            copy.start()

    late_loads = [
        pltpu.make_async_copy(src, dst, load_sem.at[3 + i])
        for i, (src, dst) in enumerate(
            ((fm_hbm, fm), (sm_hbm, sm), (gm_hbm, masters.at[0, :, own_lanes]), (om_hbm, masters.at[1, :, own_lanes]))
        )
    ]
    for copy in late_loads:
        copy.start()

    def line_signal(r):
        for peer in z_neighbours:
            pl.semaphore_signal(line_sem.at[r], inc=1, device_id=peer, device_id_type=MESH)

    def line_wait(r):
        pl.semaphore_wait(line_sem.at[r], 2)

    def arrived(like, sem):
        pltpu.make_async_copy(like, like, sem).wait()

    hk, half_rank = rk // 2, rank // 2
    natural = lax.broadcasted_iota(jnp.int32, (rank, rank), 0)
    place = lax.broadcasted_iota(jnp.int32, (rank, rank), 1)
    inner = lax.rem(place, half_rank)
    wanted = lax.div(inner, hk) * rk + lax.div(place, half_rank) * hk + lax.rem(inner, hk)
    order = jnp.where(natural == wanted, 1.0, 0.0).astype(BF16)
    proj_load.wait()
    slab = jnp.where(c == 0, proj[:, 0, :], proj[:, 1, :])
    slab = jnp.dot(slab, order, preferred_element_type=F32).astype(BF16)
    for h in range(2):
        pfull[h, own_lanes, :] = slab[:, h * half_rank : (h + 1) * half_rank]
    pl.semaphore_wait(barrier, len(greeted))
    line_signal(0)

    def p_copy(h, src, first, count, recv, peer):
        at = pl.ds(pl.multiple_of(src * rows + first, count), count)
        return pltpu.make_async_remote_copy(
            pfull.at[h, at], pfull.at[h, at], p_send.at[h], recv, device_id=peer, device_id_type=MESH
        )

    hr = rows // 2
    for h in range(2):
        for d in axis_offsets:
            p_copy(h, fs, 0, rows, pf_recv.at[h, d], fs_peer(d)).start()

    @pl.when(c == 0)
    def _():
        for copy in swaps(b_hbm, cv_hbm):
            copy.start()

    @pl.when(c == 1)
    def _():
        for copy in swaps(x_hbm, g_hbm):
            copy.start()

    for h in range(2):
        for k in range(1, max(NX, NY)):
            if k < NX:
                p_copy(h, fs_source(k), 0, rows, pf_recv.at[h, k], fs_peer(k)).wait_recv()
                for j in y_offsets:
                    p_copy(h, fs_source(k), 0, hr, pd_recv.at[h, j], fs_peer(j * NX)).start()
            if k < NY:
                p_copy(h, fs_source(k * NX), 0, rows, pf_recv.at[h, k * NX], fs_peer(k * NX)).wait_recv()
                for j in x_offsets:
                    p_copy(h, fs_source(k * NX), hr, hr, pd_recv.at[h, k], fs_peer(j)).start()

    line_wait(0)
    line_signal(1)
    for copy in own_loads(x_hbm, g_hbm):
        copy.wait()
    for copy in swaps(x_hbm, g_hbm):
        copy.wait_recv()

    def rs_copy(h, d, dst):
        return pltpu.make_async_remote_copy(
            lowb.at[h, dst], rs.at[h, d], rs_send.at[h], rs_recv.at[h], device_id=fs_peer(d), device_id_type=MESH
        )

    def fs_target(d):
        return lax.rem(y + d // NX, NY) * NX + lax.rem(x + d % NX, NX)

    turn = (((0,), (0,)), ((), ()))
    for h in range(2):
        for dy in range(NY):
            if dy > 0:
                arrived(pfull.at[h, pl.ds(0, (NX - 1) * rows)], pd_recv.at[h, dy])
            ydim = lax.rem(y + NY - dy, NY)
            at = pl.ds(pl.multiple_of(ydim * (NX * rows), NX * rows), NX * rows)
            for s in range(2):
                term = jnp.dot(ax[s, :, at], pfull[h, at, :], preferred_element_type=F32)
                span = pl.ds(s * tokens, tokens)
                if dy == 0:
                    mix[span, :] = term
                else:
                    mix[span, :] += term

        both = mix[...]
        upper = both.astype(BF16)
        lower = (both - upper.astype(F32)).astype(BF16)
        cots = ag[...].reshape(2 * tokens, ag.shape[-1])
        part = lax.dot_general(upper, cots, turn, preferred_element_type=F32) + lax.dot_general(
            lower, cots, turn, preferred_element_type=F32
        )
        low[h] = part.reshape(NFS, hk, part.shape[-1])
        lowb[h] = low[h].astype(BF16)
        for d in fs_offsets:
            rs_copy(h, d, fs_target(d)).start()
        line_wait(1 + h)
        line_signal(2 + h)

    po_copy = pltpu.make_async_remote_copy(
        pfull, pfull, po_sem.at[0], po_sem.at[1], device_id=partner, device_id_type=MESH
    )
    po_copy.start()

    sums = []
    for h in range(2):
        total = low[h, fs]
        arrived(rs.at[h, pl.ds(1, NFS - 1)], rs_recv.at[h])
        for d in range(1, NFS):
            total = total + rs[h, d].astype(F32)
        sums.append(total)
    top, bottom = sums
    left = lax.rem(lax.broadcasted_iota(jnp.int32, top.shape, 1), width) < half
    psf[0] = jnp.where(left, top, pltpu.roll(bottom, half, 1))
    psf[1] = jnp.where(left, pltpu.roll(top, top.shape[1] - half, 1), bottom)
    psb[...] = psf[...].astype(BF16)

    def z_copy(e):
        zt = lax.rem(z + e // 2, NZ)
        return pltpu.make_async_remote_copy(
            psb.at[lax.rem(c + e % 2, 2), :, pl.ds(pl.multiple_of(zt * width, width), width)],
            zb.at[e],
            z_send,
            z_recv,
            device_id=tp_peer(e),
            device_id_type=MESH,
        )

    line_wait(3)
    for e in tp_offsets:
        z_copy(e).start()

    for copy in late_loads:
        copy.wait()

    def m_copy(m, src, send, recv, peer):
        at = pl.ds(pl.multiple_of(src * rows, rows), rows)
        return pltpu.make_async_remote_copy(
            masters.at[m, :, at], masters.at[m, :, at], send, recv, device_id=peer, device_id_type=MESH
        )

    for d in axis_offsets:
        for m in range(2):
            m_copy(m, fs, mf_send, mf_recv, fs_peer(d)).start()

    same = psf[c, :, pl.ds(pl.multiple_of(z * width, width), width)]
    other = jnp.zeros_like(same)
    arrived(zb.at[pl.ds(1, 2 * NZ - 1)], z_recv)
    for e in range(1, 2 * NZ):
        if e % 2:
            other = other + zb[e].astype(F32)
        else:
            same = same + zb[e].astype(F32)

    fm_in, sm_in = fm[...], sm[...]
    directions = []
    for m in range(2):
        packed = jnp.where(c == m, same, other)
        part = jnp.concatenate([packed[:, :half], packed[:, half:]], axis=0)
        first = BETA_FIRST * fm_in[:, m, :] + (1.0 - BETA_FIRST) * part
        second = BETA_SECOND * sm_in[:, m, :] + (1.0 - BETA_SECOND) * part * part
        fn_out[:, m, :] = first
        sn_out[:, m, :] = second
        directions.append(first / jnp.sqrt(second))
    mine = pl.ds(pl.multiple_of(fs * rk, rk), rk)
    dall[mine, :] = jnp.concatenate(directions, axis=1).astype(BF16)

    def d_copy(d):
        at = pl.ds(pl.multiple_of(fs * rk, rk), rk)
        return pltpu.make_async_remote_copy(
            dall.at[at], dall.at[at], d_send, d_recv, device_id=fs_peer(d), device_id_type=MESH
        )

    for d in fs_offsets:
        d_copy(d).start()

    arrived(masters.at[:, :, pl.ds(0, len(axis_offsets) * rows)], mf_recv)
    for k in range(1, NX):
        for j in y_offsets:
            m_copy(0, fs_source(k), md_send, md_recv, fs_peer(j * NX)).start()
    for k in range(1, NY):
        for j in x_offsets:
            m_copy(1, fs_source(k * NX), md_send, md_recv, fs_peer(j)).start()

    arrived(dall.at[pl.ds(0, (NFS - 1) * rk)], d_recv)

    rotated = dall[...]
    wide = rotated.astype(F32)
    cb[0] = jnp.sum(wide * wide, axis=0, keepdims=True)

    def c_copy(e):
        return pltpu.make_async_remote_copy(
            cb.at[0], cb.at[e], c_send, c_recv, device_id=tp_peer(e), device_id_type=MESH
        )

    for e in tp_offsets:
        c_copy(e).start()

    po_copy.wait_recv()
    turned = lax.dot_general(rotated, order, turn, preferred_element_type=F32).astype(BF16)
    for m in range(2):
        lhs = turned[m * half : (m + 1) * half]
        across = (((1,), (1,)), ((), ()))
        raws[m] = lax.dot_general(
            lhs[:, :half_rank], pboth[m, 0], across, preferred_element_type=F32
        ) + lax.dot_general(lhs[:, half_rank:], pboth[m, 1], across, preferred_element_type=F32)

    squares = cb[0]
    arrived(cb.at[pl.ds(1, 2 * NZ - 1)], c_recv)
    for e in range(1, 2 * NZ):
        squares = squares + cb[e]
    clip_level = CLIP_SHARE * math.sqrt(rank * width * NZ)
    factors = []
    for m in range(2):
        norm = jnp.sqrt(jnp.sum(squares[:, m * half : (m + 1) * half], axis=(0, 1), keepdims=True))
        factors.append(clip_level / jnp.maximum(norm, clip_level))
    steps = (sg_out, so_out)
    news = (gn_out, on_out)
    for m in range(2):
        step = raws[m, :, own_lanes] * factors[m]
        steps[m][...] = step
        news[m][...] = masters[m, :, own_lanes] - LEARN_RATE * step
    diagonal = (NY - 1) * (NX - 1)
    arrived(masters.at[:, :, pl.ds(0, diagonal * rows)], md_recv)
    for m in range(2):
        ebuf[m] = (masters[m] - LEARN_RATE * (raws[m] * factors[m])).astype(BF16)

    for h in range(2):
        arrived(pfull.at[h, pl.ds(0, (NFS - 1) * rows)], p_send.at[h])
        arrived(rs.at[h, pl.ds(1, NFS - 1)], rs_send.at[h])
    po_copy.wait_send()
    arrived(zb.at[pl.ds(1, 2 * NZ - 1)], z_send)
    arrived(masters.at[:, :, pl.ds(0, len(axis_offsets) * rows)], mf_send)
    arrived(dall.at[pl.ds(0, (NFS - 1) * rk)], d_send)
    arrived(masters.at[:, :, pl.ds(0, diagonal * rows)], md_send)
    arrived(cb.at[pl.ds(1, 2 * NZ - 1)], c_send)
    for copy in swaps(x_hbm, g_hbm):
        copy.wait_send()


def store_kernel(*refs):
    count = (len(refs) - 2) // 2
    ins, outs, sem = refs[:count], refs[count:-1], refs[-1]
    sources = [*ins[:-1], ins[-1].at[0], ins[-1].at[1]]
    copies = [pltpu.make_async_copy(src, dst, sem.at[i]) for i, (src, dst) in enumerate(zip(sources, outs))]
    for copy in copies:
        copy.start()
    for copy in copies:
        copy.wait()


def shards(sizes, x, g, cv, b, proj, fm, sm, gm, om):
    NY, NX, NZ = sizes
    NFS = NY * NX
    tokens, d_model = x.shape
    channels = g.shape[1]
    rows, _, rank = proj.shape
    rk = rank // NFS
    cols = gm.shape[1]
    width = 2 * cols
    vmem = pl.BlockSpec(memory_space=pltpu.VMEM)
    hbm = pl.BlockSpec(memory_space=pltpu.HBM)
    dma = pltpu.SemaphoreType.DMA
    small = jax.ShapeDtypeStruct(fm.shape, F32)
    block = jax.ShapeDtypeStruct((cols, rows), F32)
    copy = jax.ShapeDtypeStruct((cols, d_model), BF16)
    results = pl.pallas_call(
        functools.partial(kernel, sizes),
        out_shape=(small, small, block, block, block, block, jax.ShapeDtypeStruct((2, cols, d_model), BF16)),
        in_specs=[hbm] * 9,
        out_specs=(vmem,) * 7,
        scratch_shapes=[
            pltpu.VMEM(proj.shape, BF16),
            pltpu.VMEM(fm.shape, F32),
            pltpu.VMEM(sm.shape, F32),
            pltpu.VMEM((2, tokens, d_model), BF16),
            pltpu.VMEM((2, tokens, channels), BF16),
            pltpu.VMEM((2, 2, d_model, rank // 2), BF16),
            pltpu.VMEM((2, cols, d_model), F32),
            pltpu.VMEM((2, cols, d_model), F32),
            pltpu.VMEM((2 * tokens, rank // 2), F32),
            pltpu.VMEM((2, NFS, rk // 2, channels), F32),
            pltpu.VMEM((2, NFS, rk // 2, channels), BF16),
            pltpu.VMEM((2, NFS, rk // 2, channels), BF16),
            pltpu.VMEM((2, rk // 2, channels), F32),
            pltpu.VMEM((2, rk // 2, channels), BF16),
            pltpu.VMEM((2 * NZ, rk // 2, width), BF16),
            pltpu.VMEM((rank, width), BF16),
            pltpu.VMEM((2 * NZ, 1, width), F32),
            dma((7,)),
            dma((2,)),
            dma((2,)),
        ]
        + [dma((2,)), dma((2, NFS)), dma((2, NY))]
        + [dma((2,))] * 2
        + [dma] * 6
        + [dma((2,))]
        + [dma] * 4
        + [pltpu.SemaphoreType.REGULAR((4,))],
        compiler_params=pltpu.CompilerParams(collective_id=0, has_side_effects=True, vmem_limit_bytes=48 * 2**20),
    )(*(pltpu.with_memory_space_constraint(a, pltpu.HBM) for a in (x, g, cv, b, proj, fm, sm, gm.T, om)))
    fn, sn, sg, so, gn, on, gc, oc = pl.pallas_call(
        store_kernel,
        out_shape=(small, small, block, block, block, block, copy, copy),
        in_specs=[vmem] * 7,
        out_specs=(hbm,) * 8,
        scratch_shapes=[dma((8,))],
        compiler_params=pltpu.CompilerParams(vmem_limit_bytes=2**20),
    )(*results)
    return fn, sn, sg.T, so, gn.T, on, gc.T, oc


def solution(mesh):
    sizes = (4, 4, 8)
    split = Mesh(mesh.devices.reshape(*sizes, 2), FS_TP)
    return build(split, sizes)


def build(split, sizes):
    in_specs = (
        P(FS_TP, None),
        P(FS_TP, None),
        P(FS_TP, None),
        P(FS_TP, None),
        P(FS, None, None),
        P(FS, None, TP),
        P(FS, None, TP),
        P(FS, TP),
        P(TP, FS),
    )
    out_specs = (
        P(FS, None, TP),
        P(FS, None, TP),
        P(FS, TP),
        P(TP, FS),
        P(FS, TP),
        P(TP, FS),
        P(None, TP),
        P(TP, None),
    )
    return jax.shard_map(
        functools.partial(shards, sizes), mesh=split, in_specs=in_specs, out_specs=out_specs, check_vma=False
    )
```

time: 49.6 us -> 45.2 us (0.911)
  Pallas kernels: 48.9 us -> 44.4 us
    pallas_call x1, Pallas kernels: 47.9 us -> 43.5 us  [shards(): pl.pallas_call(functools.partial(kernel, sizes), out_shape=(small, small,...]
where the time goes in v4:
time: 45.2 us; the launch traced here: 45.1 us
  Pallas kernels  44.4 us (98%)
  between operations  0.64 us (1%)
    pallas_call x1, Pallas kernels, shards(): pl.pallas_call(functools.partial(kernel, sizes), out_shape=(small, small,...  43.5 us
    pallas_call x1, Pallas kernels, shards(): pl.pallas_call(store_kernel, out_shape=(small, small, block, block, block...  0.92 us

profile of v4, /device:TPU:1, one launch (start us, length us, event | category | flops | bytes accessed | tf_op | source)
XLA Modules:
  0.0 45.1 jit_solution(5085423138625751215)
XLA Ops:
  0.6 43.5 %shard_map.152 = (f32[16,2,64]{2,1,0:T(2,128)S(1)}, f32[16,2,64]{2,1,0:T(2,128)S(1)}, f32[64,128]{1,0:T(8,128)S(1)}, f32[64,128]{1,0:T(8,128)S(1)}, f32[64,128]{...) custom-call(bf16[256,2048]{1,0:T(8,128)(2,1)} %x_hbm.1, bf16[256,1024]{1,0:T(8,128)(2,1)} %g_hbm.1, ...), custom_call_target="tpu_custom_call" | custom-call | tf_op jit(solution)/shard_map/pallas_call | solution.py:426
  44.2 0.9 %shard_map.153 = (f32[16,2,64]{2,1,0:T(2,128)}, f32[16,2,64]{2,1,0:T(2,128)}, f32[64,128]{1,0:T(8,128)}, f32[64,128]{1,0:T(8,128)}, f32[64,128]{1,0:T(8,128)}, /...) custom-call(f32[16,2,64]{2,1,0:T(2,128)S(1)} %get-tuple-element.23.refs_0_, ...), custom_call_target="tpu_custom_call" | custom-call | tf_op jit(solution)/shard_map/pallas_call | solution.py:461

commit v5 on v4

--- a/solution.py
+++ b/solution.py
@@ -82,7 +82,7 @@
     NFS = NY * NX
     tokens = x_hbm.shape[0]
     rows = proj.shape[0]
-    rank = 2 * pboth.shape[3]
+    rank = 2 * pboth.shape[2]
     rk = rank // NFS
     width = zb.shape[-1]
     half = width // 2
@@ -131,8 +131,9 @@
     proj_load = pltpu.make_async_copy(proj_hbm, proj, load_sem.at[2])
     proj_load.start()
     axis_offsets = [k for k in range(1, NX)] + [k * NX for k in range(1, NY)]
-    z_neighbours = ((y, x, lax.rem(z + 1, NZ), c), (y, x, lax.rem(z + NZ - 1, NZ), c))
-    greeted = [fs_peer(d) for d in axis_offsets] + [partner, *z_neighbours]
+    near = [k for k in range(1, NZ) if hops(k, NZ) <= 2]
+    relays = [(y, x, lax.rem(z + k, NZ), c) for k in near if hops(k, NZ) == 2]
+    greeted = [fs_peer(d) for d in axis_offsets] + [partner] + [tp_peer(2 * k + i) for k in near for i in range(2)]
     barrier = pltpu.get_barrier_semaphore()
     for peer in greeted:
         pl.semaphore_signal(barrier, inc=1, device_id=peer, device_id_type=MESH)
@@ -155,13 +156,6 @@
     ]
     for copy in late_loads:
         copy.start()
-
-    def line_signal(r):
-        for peer in z_neighbours:
-            pl.semaphore_signal(line_sem.at[r], inc=1, device_id=peer, device_id_type=MESH)
-
-    def line_wait(r):
-        pl.semaphore_wait(line_sem.at[r], 2)
 
     def arrived(like, sem):
         pltpu.make_async_copy(like, like, sem).wait()
@@ -174,22 +168,36 @@
     order = jnp.where(natural == wanted, 1.0, 0.0).astype(BF16)
     proj_load.wait()
     slab = jnp.where(c == 0, proj[:, 0, :], proj[:, 1, :])
-    slab = jnp.dot(slab, order, preferred_element_type=F32).astype(BF16)
+    slab = lax.dot_general(order, slab, (((0,), (1,)), ((), ())), preferred_element_type=F32).astype(BF16)
     for h in range(2):
-        pfull[h, own_lanes, :] = slab[:, h * half_rank : (h + 1) * half_rank]
+        pfull[h, :, own_lanes] = slab[h * half_rank : (h + 1) * half_rank]
     pl.semaphore_wait(barrier, len(greeted))
-    line_signal(0)
+    for peer in relays:
+        pl.semaphore_signal(line_sem, inc=1, device_id=peer, device_id_type=MESH)
 
     def p_copy(h, src, first, count, recv, peer):
-        at = pl.ds(pl.multiple_of(src * rows + first, count), count)
-        return pltpu.make_async_remote_copy(
-            pfull.at[h, at], pfull.at[h, at], p_send.at[h], recv, device_id=peer, device_id_type=MESH
-        )
-
-    hr = rows // 2
-    for h in range(2):
+        at = pl.ds(pl.multiple_of(src * rows, rows), rows)
+        ref = pfull.at[h, pl.ds(first, count), at]
+        return pltpu.make_async_remote_copy(ref, ref, p_send.at[h], recv, device_id=peer, device_id_type=MESH)
+
+    hr = half_rank // 2
+
+    def p_first(h):
         for d in axis_offsets:
-            p_copy(h, fs, 0, rows, pf_recv.at[h, d], fs_peer(d)).start()
+            p_copy(h, fs, 0, half_rank, pf_recv.at[h, axis_offsets.index(d)], fs_peer(d)).start()
+
+    def p_onward(h, k):
+        if k < NX:
+            p_copy(h, fs_source(k), 0, half_rank, pf_recv.at[h, axis_offsets.index(k)], fs_peer(k)).wait_recv()
+            for j in y_offsets:
+                p_copy(h, fs_source(k), 0, hr, pd_recv.at[h, j], fs_peer(j * NX)).start()
+        if k < NY:
+            sem = pf_recv.at[h, axis_offsets.index(k * NX)]
+            p_copy(h, fs_source(k * NX), 0, half_rank, sem, fs_peer(k * NX)).wait_recv()
+            for j in x_offsets:
+                p_copy(h, fs_source(k * NX), hr, hr, pd_recv.at[h, k], fs_peer(j)).start()
+
+    p_first(0)
 
     @pl.when(c == 0)
     def _():
@@ -201,19 +209,12 @@
         for copy in swaps(x_hbm, g_hbm):
             copy.start()
 
+    steps = sorted(range(1, max(NX, NY)), key=lambda k: hops(k, max(NX, NY)))
+    p_first(1)
     for h in range(2):
-        for k in range(1, max(NX, NY)):
-            if k < NX:
-                p_copy(h, fs_source(k), 0, rows, pf_recv.at[h, k], fs_peer(k)).wait_recv()
-                for j in y_offsets:
-                    p_copy(h, fs_source(k), 0, hr, pd_recv.at[h, j], fs_peer(j * NX)).start()
-            if k < NY:
-                p_copy(h, fs_source(k * NX), 0, rows, pf_recv.at[h, k * NX], fs_peer(k * NX)).wait_recv()
-                for j in x_offsets:
-                    p_copy(h, fs_source(k * NX), hr, hr, pd_recv.at[h, k], fs_peer(j)).start()
-
-    line_wait(0)
-    line_signal(1)
+        for k in steps:
+            p_onward(h, k)
+
     for copy in own_loads(x_hbm, g_hbm):
         copy.wait()
     for copy in swaps(x_hbm, g_hbm):
@@ -227,34 +228,37 @@
     def fs_target(d):
         return lax.rem(y + d // NX, NY) * NX + lax.rem(x + d % NX, NX)
 
-    turn = (((0,), (0,)), ((), ()))
+    across = (((1,), (1,)), ((), ()))
+
+    def mix_slabs(h, dy):
+        if dy > 0:
+            arrived(pfull.at[h, :, pl.ds(0, (NX - 1) * rows)], pd_recv.at[h, dy])
+        ydim = lax.rem(y + NY - dy, NY)
+        at = pl.ds(pl.multiple_of(ydim * (NX * rows), NX * rows), NX * rows)
+        for s in range(2):
+            term = lax.dot_general(pfull[h, :, at], ax[s, :, at], across, preferred_element_type=F32)
+            span = slice(s * tokens, (s + 1) * tokens)
+            if dy == 0:
+                mix[h, :, span] = term
+            else:
+                mix[h, :, span] += term
+
     for h in range(2):
-        for dy in range(NY):
-            if dy > 0:
-                arrived(pfull.at[h, pl.ds(0, (NX - 1) * rows)], pd_recv.at[h, dy])
-            ydim = lax.rem(y + NY - dy, NY)
-            at = pl.ds(pl.multiple_of(ydim * (NX * rows), NX * rows), NX * rows)
-            for s in range(2):
-                term = jnp.dot(ax[s, :, at], pfull[h, at, :], preferred_element_type=F32)
-                span = pl.ds(s * tokens, tokens)
-                if dy == 0:
-                    mix[span, :] = term
-                else:
-                    mix[span, :] += term
-
-        both = mix[...]
+        mix_slabs(h, 0)
+    cots = ag[...].reshape(2 * tokens, ag.shape[-1])
+    for h in range(2):
+        for dy in range(1, NY):
+            mix_slabs(h, dy)
+
+        both = mix[h]
         upper = both.astype(BF16)
         lower = (both - upper.astype(F32)).astype(BF16)
-        cots = ag[...].reshape(2 * tokens, ag.shape[-1])
-        part = lax.dot_general(upper, cots, turn, preferred_element_type=F32) + lax.dot_general(
-            lower, cots, turn, preferred_element_type=F32
-        )
+        pair = jnp.dot(jnp.concatenate([upper, lower], axis=0), cots, preferred_element_type=F32)
+        part = pair[:half_rank] + pair[half_rank:]
         low[h] = part.reshape(NFS, hk, part.shape[-1])
         lowb[h] = low[h].astype(BF16)
         for d in fs_offsets:
             rs_copy(h, d, fs_target(d)).start()
-        line_wait(1 + h)
-        line_signal(2 + h)
 
     po_copy = pltpu.make_async_remote_copy(
         pfull, pfull, po_sem.at[0], po_sem.at[1], device_id=partner, device_id_type=MESH
@@ -285,7 +289,7 @@
             device_id_type=MESH,
         )
 
-    line_wait(3)
+    pl.semaphore_wait(line_sem, len(relays))
     for e in tp_offsets:
         z_copy(e).start()
 
@@ -356,13 +360,13 @@
         c_copy(e).start()
 
     po_copy.wait_recv()
-    turned = lax.dot_general(rotated, order, turn, preferred_element_type=F32).astype(BF16)
+    turned = lax.dot_general(rotated, order, (((0,), (0,)), ((), ())), preferred_element_type=F32).astype(BF16)
     for m in range(2):
-        lhs = turned[m * half : (m + 1) * half]
-        across = (((1,), (1,)), ((), ()))
-        raws[m] = lax.dot_general(
-            lhs[:, :half_rank], pboth[m, 0], across, preferred_element_type=F32
-        ) + lax.dot_general(lhs[:, half_rank:], pboth[m, 1], across, preferred_element_type=F32)
+        raws[m] = jnp.dot(
+            turned[m * half : (m + 1) * half],
+            pboth[m].reshape(rank, pboth.shape[-1]),
+            preferred_element_type=F32,
+        )
 
     squares = cb[0]
     arrived(cb.at[pl.ds(1, 2 * NZ - 1)], c_recv)
@@ -385,7 +389,7 @@
         ebuf[m] = (masters[m] - LEARN_RATE * (raws[m] * factors[m])).astype(BF16)
 
     for h in range(2):
-        arrived(pfull.at[h, pl.ds(0, (NFS - 1) * rows)], p_send.at[h])
+        arrived(pfull.at[h, :, pl.ds(0, (NFS - 1) * rows)], p_send.at[h])
         arrived(rs.at[h, pl.ds(1, NFS - 1)], rs_send.at[h])
     po_copy.wait_send()
     arrived(zb.at[pl.ds(1, 2 * NZ - 1)], z_send)
@@ -434,10 +438,10 @@
             pltpu.VMEM(sm.shape, F32),
             pltpu.VMEM((2, tokens, d_model), BF16),
             pltpu.VMEM((2, tokens, channels), BF16),
-            pltpu.VMEM((2, 2, d_model, rank // 2), BF16),
+            pltpu.VMEM((2, 2, rank // 2, d_model), BF16),
             pltpu.VMEM((2, cols, d_model), F32),
             pltpu.VMEM((2, cols, d_model), F32),
-            pltpu.VMEM((2 * tokens, rank // 2), F32),
+            pltpu.VMEM((2, rank // 2, 2 * tokens), F32),
             pltpu.VMEM((2, NFS, rk // 2, channels), F32),
             pltpu.VMEM((2, NFS, rk // 2, channels), BF16),
             pltpu.VMEM((2, NFS, rk // 2, channels), BF16),
@@ -450,12 +454,12 @@
             dma((2,)),
             dma((2,)),
         ]
-        + [dma((2,)), dma((2, NFS)), dma((2, NY))]
+        + [dma((2,)), dma((2, NX + NY - 2)), dma((2, NY))]
         + [dma((2,))] * 2
         + [dma] * 6
         + [dma((2,))]
         + [dma] * 4
-        + [pltpu.SemaphoreType.REGULAR((4,))],
+        + [pltpu.SemaphoreType.REGULAR],
         compiler_params=pltpu.CompilerParams(collective_id=0, has_side_effects=True, vmem_limit_bytes=48 * 2**20),
     )(*(pltpu.with_memory_space_constraint(a, pltpu.HBM) for a in (x, g, cv, b, proj, fm, sm, gm.T, om)))
     fn, sn, sg, so, gn, on, gc, oc = pl.pallas_call(

time: 45.2 us -> 43.5 us (0.962)
  Pallas kernels: 44.4 us -> 42.8 us
    pallas_call x1, Pallas kernels: 43.5 us -> 41.8 us  [shards(): pl.pallas_call(functools.partial(kernel, sizes), out_shape=(small, small,...]
where the time goes in v5:
time: 43.5 us; the launch traced here: 43.4 us
  Pallas kernels  42.8 us (98%)
  between operations  0.64 us (1%)
    pallas_call x1, Pallas kernels, shards(): pl.pallas_call(functools.partial(kernel, sizes), out_shape=(small, small,...  41.8 us
    pallas_call x1, Pallas kernels, shards(): pl.pallas_call(store_kernel, out_shape=(small, small, block, block, block...  0.92 us

profile of v5, /device:TPU:1, one launch (start us, length us, event | category | flops | bytes accessed | tf_op | source)
XLA Modules:
  0.0 43.4 jit_solution(7618946581583718532)
XLA Ops:
  0.6 41.8 %shard_map.152 = (f32[16,2,64]{2,1,0:T(2,128)S(1)}, f32[16,2,64]{2,1,0:T(2,128)S(1)}, f32[64,128]{1,0:T(8,128)S(1)}, f32[64,128]{1,0:T(8,128)S(1)}, f32[64,128]{...) custom-call(bf16[256,2048]{1,0:T(8,128)(2,1)} %x_hbm.1, bf16[256,1024]{1,0:T(8,128)(2,1)} %g_hbm.1, ...), custom_call_target="tpu_custom_call" | custom-call | tf_op jit(solution)/shard_map/pallas_call | solution.py:430
  42.5 0.9 %shard_map.153 = (f32[16,2,64]{2,1,0:T(2,128)}, f32[16,2,64]{2,1,0:T(2,128)}, f32[64,128]{1,0:T(8,128)}, f32[64,128]{1,0:T(8,128)}, f32[64,128]{1,0:T(8,128)}, /...) custom-call(f32[16,2,64]{2,1,0:T(2,128)S(1)} %get-tuple-element.23.refs_0_, ...), custom_call_target="tpu_custom_call" | custom-call | tf_op jit(solution)/shard_map/pallas_call | solution.py:465

commit v6 on v5

--- a/solution.py
+++ b/solution.py
@@ -57,6 +57,7 @@
     zb,
     dall,
     cb,
+    fx,
     load_sem,
     swap_send,
     swap_recv,
@@ -77,6 +78,9 @@
     md_send,
     md_recv,
     line_sem,
+    moment_send,
+    moment_recv,
+    back_sem,
 ):
     NY, NX, NZ = sizes
     NFS = NY * NX
@@ -108,7 +112,7 @@
         return min(k, n - k)
 
     fs_offsets = sorted(range(1, NFS), key=lambda d: -hops(d // NX, NY) - hops(d % NX, NX))
-    tp_offsets = sorted(range(1, 2 * NZ), key=lambda e: -2 * hops(e // 2, NZ) - e % 2)
+    z_offsets = sorted(range(1, NZ), key=lambda k: -hops(k, NZ))
     y_offsets = sorted(range(1, NY), key=lambda j: -hops(j, NY))
     x_offsets = sorted(range(1, NX), key=lambda j: -hops(j, NX))
 
@@ -151,7 +155,7 @@
     late_loads = [
         pltpu.make_async_copy(src, dst, load_sem.at[3 + i])
         for i, (src, dst) in enumerate(
-            ((fm_hbm, fm), (sm_hbm, sm), (gm_hbm, masters.at[0, :, own_lanes]), (om_hbm, masters.at[1, :, own_lanes]))
+            ((fm_hbm, fm.at[c]), (sm_hbm, sm.at[c]), (gm_hbm, masters.at[0, :, own_lanes]), (om_hbm, masters.at[1, :, own_lanes]))
         )
     ]
     for copy in late_loads:
@@ -197,11 +201,18 @@
             for j in x_offsets:
                 p_copy(h, fs_source(k * NX), hr, hr, pd_recv.at[h, k], fs_peer(j)).start()
 
+    moment_copies = tuple(
+        pltpu.make_async_remote_copy(
+            src, dst.at[0], moment_send.at[i], moment_recv.at[i], device_id=partner, device_id_type=MESH
+        )
+        for i, (src, dst) in enumerate(((fm_hbm, fm), (sm_hbm, sm)))
+    )
+
     p_first(0)
 
     @pl.when(c == 0)
     def _():
-        for copy in swaps(b_hbm, cv_hbm):
+        for copy in swaps(b_hbm, cv_hbm) + moment_copies:
             copy.start()
 
     @pl.when(c == 1)
@@ -265,6 +276,22 @@
     )
     po_copy.start()
 
+    for copy in late_loads:
+        copy.wait()
+
+    def m_copy(m, src, send, recv, peer):
+        at = pl.ds(pl.multiple_of(src * rows, rows), rows)
+        return pltpu.make_async_remote_copy(
+            masters.at[m, :, at], masters.at[m, :, at], send, recv, device_id=peer, device_id_type=MESH
+        )
+
+    def m_first():
+        for d in axis_offsets:
+            for m in range(2):
+                m_copy(m, fs, mf_send, mf_recv, fs_peer(d)).start()
+
+    pl.when(c == 0)(m_first)
+
     sums = []
     for h in range(2):
         total = low[h, fs]
@@ -272,110 +299,123 @@
         for d in range(1, NFS):
             total = total + rs[h, d].astype(F32)
         sums.append(total)
-    top, bottom = sums
-    left = lax.rem(lax.broadcasted_iota(jnp.int32, top.shape, 1), width) < half
-    psf[0] = jnp.where(left, top, pltpu.roll(bottom, half, 1))
-    psf[1] = jnp.where(left, pltpu.roll(top, top.shape[1] - half, 1), bottom)
-    psb[...] = psf[...].astype(BF16)
-
-    def z_copy(e):
-        zt = lax.rem(z + e // 2, NZ)
+    for h in range(2):
+        psf[h] = sums[h]
+        psb[h] = sums[h].astype(BF16)
+
+    def z_copy(dz):
+        zt = lax.rem(z + dz, NZ)
         return pltpu.make_async_remote_copy(
-            psb.at[lax.rem(c + e % 2, 2), :, pl.ds(pl.multiple_of(zt * width, width), width)],
-            zb.at[e],
+            psb.at[:, :, pl.ds(pl.multiple_of(zt * width, width), width)],
+            zb.at[2 * dz + c],
             z_send,
             z_recv,
-            device_id=tp_peer(e),
+            device_id=(y, x, zt, 1),
             device_id_type=MESH,
         )
 
     pl.semaphore_wait(line_sem, len(relays))
-    for e in tp_offsets:
-        z_copy(e).start()
-
-    for copy in late_loads:
-        copy.wait()
-
-    def m_copy(m, src, send, recv, peer):
-        at = pl.ds(pl.multiple_of(src * rows, rows), rows)
-        return pltpu.make_async_remote_copy(
-            masters.at[m, :, at], masters.at[m, :, at], send, recv, device_id=peer, device_id_type=MESH
-        )
-
-    for d in axis_offsets:
-        for m in range(2):
-            m_copy(m, fs, mf_send, mf_recv, fs_peer(d)).start()
-
-    same = psf[c, :, pl.ds(pl.multiple_of(z * width, width), width)]
-    other = jnp.zeros_like(same)
-    arrived(zb.at[pl.ds(1, 2 * NZ - 1)], z_recv)
-    for e in range(1, 2 * NZ):
-        if e % 2:
-            other = other + zb[e].astype(F32)
-        else:
-            same = same + zb[e].astype(F32)
-
-    fm_in, sm_in = fm[...], sm[...]
-    directions = []
-    for m in range(2):
-        packed = jnp.where(c == m, same, other)
-        part = jnp.concatenate([packed[:, :half], packed[:, half:]], axis=0)
-        first = BETA_FIRST * fm_in[:, m, :] + (1.0 - BETA_FIRST) * part
-        second = BETA_SECOND * sm_in[:, m, :] + (1.0 - BETA_SECOND) * part * part
-        fn_out[:, m, :] = first
-        sn_out[:, m, :] = second
-        directions.append(first / jnp.sqrt(second))
-    mine = pl.ds(pl.multiple_of(fs * rk, rk), rk)
-    dall[mine, :] = jnp.concatenate(directions, axis=1).astype(BF16)
+    for dz in z_offsets:
+        z_copy(dz).start()
+    pl.when(c == 0)(lambda: z_copy(0).start())
+
+    pl.when(c == 1)(m_first)
 
     def d_copy(d):
         at = pl.ds(pl.multiple_of(fs * rk, rk), rk)
         return pltpu.make_async_remote_copy(
-            dall.at[at], dall.at[at], d_send, d_recv, device_id=fs_peer(d), device_id_type=MESH
-        )
-
-    for d in fs_offsets:
-        d_copy(d).start()
-
-    arrived(masters.at[:, :, pl.ds(0, len(axis_offsets) * rows)], mf_recv)
-    for k in range(1, NX):
-        for j in y_offsets:
-            m_copy(0, fs_source(k), md_send, md_recv, fs_peer(j * NX)).start()
-    for k in range(1, NY):
-        for j in x_offsets:
-            m_copy(1, fs_source(k * NX), md_send, md_recv, fs_peer(j)).start()
-
-    arrived(dall.at[pl.ds(0, (NFS - 1) * rk)], d_recv)
-
-    rotated = dall[...]
-    wide = rotated.astype(F32)
-    cb[0] = jnp.sum(wide * wide, axis=0, keepdims=True)
-
-    def c_copy(e):
+            dall.at[:, at], dall.at[:, at], d_send, d_recv, device_id=fs_peer(d), device_id_type=MESH
+        )
+
+    back_copies = (
+        pltpu.make_async_remote_copy(
+            fx.at[0], fx.at[0], back_sem.at[0], back_sem.at[1], device_id=partner, device_id_type=MESH
+        ),
+        pltpu.make_async_remote_copy(
+            dall, dall, back_sem.at[2], back_sem.at[3], device_id=partner, device_id_type=MESH
+        ),
+    )
+
+    def m_onward():
+        arrived(masters.at[:, :, pl.ds(0, len(axis_offsets) * rows)], mf_recv)
+        for k in range(1, NX):
+            for j in y_offsets:
+                m_copy(0, fs_source(k), md_send, md_recv, fs_peer(j * NX)).start()
+        for k in range(1, NY):
+            for j in x_offsets:
+                m_copy(1, fs_source(k * NX), md_send, md_recv, fs_peer(j)).start()
+
+    pl.when(c == 0)(m_onward)
+
+    @pl.when(c == 1)
+    def _():
+        for copy in moment_copies:
+            copy.wait_recv()
+        arrived(zb.at[pl.ds(0, 2 * NZ - 1)], z_recv)
+        wholes = [zb[0].astype(F32), psf[:, :, pl.ds(pl.multiple_of(z * width, width), width)]]
+        for dz in range(1, NZ):
+            for m in range(2):
+                wholes[m] = wholes[m] + zb[2 * dz + m].astype(F32)
+        for m in range(2):
+            part = wholes[m].reshape(rk, width)
+            first_in = jnp.concatenate([fm[0, :, m, :], fm[1, :, m, :]], axis=1)
+            second_in = jnp.concatenate([sm[0, :, m, :], sm[1, :, m, :]], axis=1)
+            first = BETA_FIRST * first_in + (1.0 - BETA_FIRST) * part
+            second = BETA_SECOND * second_in + (1.0 - BETA_SECOND) * part * part
+            dall[m, pl.ds(pl.multiple_of(fs * rk, rk), rk), :] = (first / jnp.sqrt(second)).astype(BF16)
+            for i in range(2):
+                fx[i, 0, :, m, :] = first[:, i * half : (i + 1) * half]
+                fx[i, 1, :, m, :] = second[:, i * half : (i + 1) * half]
+        for d in fs_offsets:
+            d_copy(d).start()
+        back_copies[0].start()
+
+    pl.when(c == 1)(m_onward)
+
+    def c_copy(dz, core):
         return pltpu.make_async_remote_copy(
-            cb.at[0], cb.at[e], c_send, c_recv, device_id=tp_peer(e), device_id_type=MESH
-        )
-
-    for e in tp_offsets:
-        c_copy(e).start()
+            cb.at[0],
+            cb.at[dz],
+            c_send,
+            c_recv,
+            device_id=(y, x, lax.rem(z + dz, NZ), core),
+            device_id_type=MESH,
+        )
+
+    @pl.when(c == 1)
+    def _():
+        arrived(dall.at[:, pl.ds(0, (NFS - 1) * rk)], d_recv)
+        for m in range(2):
+            wide = dall[m].astype(F32)
+            cb[0, pl.ds(m, 1), :] = jnp.sum(wide * wide, axis=0, keepdims=True)
+        for dz in z_offsets:
+            for core in range(2):
+                c_copy(dz, core).start()
+        c_copy(0, 0).start()
+        back_copies[1].start()
+
+    pl.when(c == 0)(lambda: back_copies[1].wait_recv())
 
     po_copy.wait_recv()
-    turned = lax.dot_general(rotated, order, (((0,), (0,)), ((), ())), preferred_element_type=F32).astype(BF16)
     for m in range(2):
+        turned = lax.dot_general(
+            dall[m], order, (((0,), (0,)), ((), ())), preferred_element_type=F32
+        ).astype(BF16)
         raws[m] = jnp.dot(
-            turned[m * half : (m + 1) * half],
+            jnp.where(c == 0, turned[:half], turned[half:]),
             pboth[m].reshape(rank, pboth.shape[-1]),
             preferred_element_type=F32,
         )
 
+    pl.when(c == 0)(lambda: arrived(cb.at[pl.ds(0, NZ)], c_recv))
+    pl.when(c == 1)(lambda: arrived(cb.at[pl.ds(1, NZ - 1)], c_recv))
     squares = cb[0]
-    arrived(cb.at[pl.ds(1, 2 * NZ - 1)], c_recv)
-    for e in range(1, 2 * NZ):
-        squares = squares + cb[e]
+    for dz in range(1, NZ):
+        squares = squares + cb[dz]
     clip_level = CLIP_SHARE * math.sqrt(rank * width * NZ)
     factors = []
     for m in range(2):
-        norm = jnp.sqrt(jnp.sum(squares[:, m * half : (m + 1) * half], axis=(0, 1), keepdims=True))
+        norm = jnp.sqrt(jnp.sum(squares[m : m + 1], axis=(0, 1), keepdims=True))
         factors.append(clip_level / jnp.maximum(norm, clip_level))
     steps = (sg_out, so_out)
     news = (gn_out, on_out)
@@ -392,11 +432,26 @@
         arrived(pfull.at[h, :, pl.ds(0, (NFS - 1) * rows)], p_send.at[h])
         arrived(rs.at[h, pl.ds(1, NFS - 1)], rs_send.at[h])
     po_copy.wait_send()
-    arrived(zb.at[pl.ds(1, 2 * NZ - 1)], z_send)
     arrived(masters.at[:, :, pl.ds(0, len(axis_offsets) * rows)], mf_send)
-    arrived(dall.at[pl.ds(0, (NFS - 1) * rk)], d_send)
     arrived(masters.at[:, :, pl.ds(0, diagonal * rows)], md_send)
-    arrived(cb.at[pl.ds(1, 2 * NZ - 1)], c_send)
+
+    @pl.when(c == 0)
+    def _():
+        arrived(zb.at[pl.ds(0, NZ)], z_send)
+        for copy in moment_copies:
+            copy.wait_send()
+        back_copies[0].wait_recv()
+
+    @pl.when(c == 1)
+    def _():
+        arrived(zb.at[pl.ds(0, NZ - 1)], z_send)
+        arrived(dall.at[:, pl.ds(0, (NFS - 1) * rk)], d_send)
+        arrived(cb.at[pl.ds(0, 2 * NZ - 1)], c_send)
+        for copy in back_copies:
+            copy.wait_send()
+
+    fn_out[...] = fx[c, 0]
+    sn_out[...] = fx[c, 1]
     for copy in swaps(x_hbm, g_hbm):
         copy.wait_send()
 
@@ -434,8 +489,8 @@
         out_specs=(vmem,) * 7,
         scratch_shapes=[
             pltpu.VMEM(proj.shape, BF16),
-            pltpu.VMEM(fm.shape, F32),
-            pltpu.VMEM(sm.shape, F32),
+            pltpu.VMEM((2, *fm.shape), F32),
+            pltpu.VMEM((2, *sm.shape), F32),
             pltpu.VMEM((2, tokens, d_model), BF16),
             pltpu.VMEM((2, tokens, channels), BF16),
             pltpu.VMEM((2, 2, rank // 2, d_model), BF16),
@@ -447,9 +502,10 @@
             pltpu.VMEM((2, NFS, rk // 2, channels), BF16),
             pltpu.VMEM((2, rk // 2, channels), F32),
             pltpu.VMEM((2, rk // 2, channels), BF16),
-            pltpu.VMEM((2 * NZ, rk // 2, width), BF16),
-            pltpu.VMEM((rank, width), BF16),
-            pltpu.VMEM((2 * NZ, 1, width), F32),
+            pltpu.VMEM((2 * NZ, 2, rk // 2, width), BF16),
+            pltpu.VMEM((2, rank, width), BF16),
+            pltpu.VMEM((2 * NZ, 2, width), F32),
+            pltpu.VMEM((2, 2, *fm.shape), F32),
             dma((7,)),
             dma((2,)),
             dma((2,)),
@@ -459,7 +515,8 @@
         + [dma] * 6
         + [dma((2,))]
         + [dma] * 4
-        + [pltpu.SemaphoreType.REGULAR],
+        + [pltpu.SemaphoreType.REGULAR]
+        + [dma((2,)), dma((2,)), dma((4,))],
         compiler_params=pltpu.CompilerParams(collective_id=0, has_side_effects=True, vmem_limit_bytes=48 * 2**20),
     )(*(pltpu.with_memory_space_constraint(a, pltpu.HBM) for a in (x, g, cv, b, proj, fm, sm, gm.T, om)))
     fn, sn, sg, so, gn, on, gc, oc = pl.pallas_call(

time: 43.5 us -> 42.2 us (0.970)
  Pallas kernels: 42.8 us -> 41.4 us
    pallas_call x1, Pallas kernels: 41.8 us -> 40.5 us  [shards(): pl.pallas_call(functools.partial(kernel, sizes), out_shape=(small, small,...]
where the time goes in v6:
time: 42.2 us; the launch traced here: 42.1 us
  Pallas kernels  41.4 us (98%)
  between operations  0.64 us (2%)
    pallas_call x1, Pallas kernels, shards(): pl.pallas_call(functools.partial(kernel, sizes), out_shape=(small, small,...  40.5 us
    pallas_call x1, Pallas kernels, shards(): pl.pallas_call(store_kernel, out_shape=(small, small, block, block, block...  0.92 us

profile of v6, /device:TPU:1, one launch (start us, length us, event | category | flops | bytes accessed | tf_op | source)
XLA Modules:
  0.0 42.1 jit_solution(7604344796189233380)
XLA Ops:
  0.6 40.5 %shard_map.152 = (f32[16,2,64]{2,1,0:T(2,128)S(1)}, f32[16,2,64]{2,1,0:T(2,128)S(1)}, f32[64,128]{1,0:T(8,128)S(1)}, f32[64,128]{1,0:T(8,128)S(1)}, f32[64,128]{...) custom-call(bf16[256,2048]{1,0:T(8,128)(2,1)} %x_hbm.1, bf16[256,1024]{1,0:T(8,128)(2,1)} %g_hbm.1, ...), custom_call_target="tpu_custom_call" | custom-call | tf_op jit(solution)/shard_map/pallas_call | solution.py:485
  41.2 0.9 %shard_map.153 = (f32[16,2,64]{2,1,0:T(2,128)}, f32[16,2,64]{2,1,0:T(2,128)}, f32[64,128]{1,0:T(8,128)}, f32[64,128]{1,0:T(8,128)}, f32[64,128]{1,0:T(8,128)}, /...) custom-call(f32[16,2,64]{2,1,0:T(2,128)S(1)} %get-tuple-element.23.refs_0_, ...), custom_call_target="tpu_custom_call" | custom-call | tf_op jit(solution)/shard_map/pallas_call | solution.py:522

commit v7 on v6

--- a/solution.py
+++ b/solution.py
@@ -231,9 +231,14 @@
     for copy in swaps(x_hbm, g_hbm):
         copy.wait_recv()
 
-    def rs_copy(h, d, dst):
+    def rs_copy(h, d):
         return pltpu.make_async_remote_copy(
-            lowb.at[h, dst], rs.at[h, d], rs_send.at[h], rs_recv.at[h], device_id=fs_peer(d), device_id_type=MESH
+            lowb.at[h, fs_target(d)],
+            rs.at[c, h, d],
+            rs_send.at[h],
+            rs_recv.at[c, h],
+            device_id=(*fs_peer(d)[:2], z, 1),
+            device_id_type=MESH,
         )
 
     def fs_target(d):
@@ -269,7 +274,8 @@
         low[h] = part.reshape(NFS, hk, part.shape[-1])
         lowb[h] = low[h].astype(BF16)
         for d in fs_offsets:
-            rs_copy(h, d, fs_target(d)).start()
+            rs_copy(h, d).start()
+        pl.when(c == 0)(lambda: rs_copy(h, 0).start())
 
     po_copy = pltpu.make_async_remote_copy(
         pfull, pfull, po_sem.at[0], po_sem.at[1], device_id=partner, device_id_type=MESH
@@ -292,22 +298,22 @@
 
     pl.when(c == 0)(m_first)
 
-    sums = []
-    for h in range(2):
-        total = low[h, fs]
-        arrived(rs.at[h, pl.ds(1, NFS - 1)], rs_recv.at[h])
-        for d in range(1, NFS):
-            total = total + rs[h, d].astype(F32)
-        sums.append(total)
-    for h in range(2):
-        psf[h] = sums[h]
-        psb[h] = sums[h].astype(BF16)
+    @pl.when(c == 1)
+    def _():
+        for m in (1, 0):
+            for h in range(2):
+                arrived(rs.at[m, h, pl.ds(m, NFS - m)], rs_recv.at[m, h])
+                total = low[h, fs] if m else rs[0, h, 0].astype(F32)
+                for d in range(1, NFS):
+                    total = total + rs[m, h, d].astype(F32)
+                psf[m, h] = total
+                psb[m, h] = total.astype(BF16)
 
     def z_copy(dz):
         zt = lax.rem(z + dz, NZ)
         return pltpu.make_async_remote_copy(
-            psb.at[:, :, pl.ds(pl.multiple_of(zt * width, width), width)],
-            zb.at[2 * dz + c],
+            psb.at[:, :, :, pl.ds(pl.multiple_of(zt * width, width), width)],
+            zb.at[dz],
             z_send,
             z_recv,
             device_id=(y, x, zt, 1),
@@ -315,11 +321,12 @@
         )
 
     pl.semaphore_wait(line_sem, len(relays))
-    for dz in z_offsets:
-        z_copy(dz).start()
-    pl.when(c == 0)(lambda: z_copy(0).start())
-
-    pl.when(c == 1)(m_first)
+
+    @pl.when(c == 1)
+    def _():
+        for dz in z_offsets:
+            z_copy(dz).start()
+        m_first()
 
     def d_copy(d):
         at = pl.ds(pl.multiple_of(fs * rk, rk), rk)
@@ -351,11 +358,11 @@
     def _():
         for copy in moment_copies:
             copy.wait_recv()
-        arrived(zb.at[pl.ds(0, 2 * NZ - 1)], z_recv)
-        wholes = [zb[0].astype(F32), psf[:, :, pl.ds(pl.multiple_of(z * width, width), width)]]
+        arrived(zb.at[pl.ds(1, NZ - 1)], z_recv)
+        wholes = [psf[m, :, :, pl.ds(pl.multiple_of(z * width, width), width)] for m in range(2)]
         for dz in range(1, NZ):
             for m in range(2):
-                wholes[m] = wholes[m] + zb[2 * dz + m].astype(F32)
+                wholes[m] = wholes[m] + zb[dz, m].astype(F32)
         for m in range(2):
             part = wholes[m].reshape(rk, width)
             first_in = jnp.concatenate([fm[0, :, m, :], fm[1, :, m, :]], axis=1)
@@ -430,20 +437,22 @@
 
     for h in range(2):
         arrived(pfull.at[h, :, pl.ds(0, (NFS - 1) * rows)], p_send.at[h])
-        arrived(rs.at[h, pl.ds(1, NFS - 1)], rs_send.at[h])
     po_copy.wait_send()
     arrived(masters.at[:, :, pl.ds(0, len(axis_offsets) * rows)], mf_send)
     arrived(masters.at[:, :, pl.ds(0, diagonal * rows)], md_send)
 
     @pl.when(c == 0)
     def _():
-        arrived(zb.at[pl.ds(0, NZ)], z_send)
+        for h in range(2):
+            arrived(rs.at[0, h], rs_send.at[h])
         for copy in moment_copies:
             copy.wait_send()
         back_copies[0].wait_recv()
 
     @pl.when(c == 1)
     def _():
+        for h in range(2):
+            arrived(rs.at[0, h, pl.ds(0, NFS - 1)], rs_send.at[h])
         arrived(zb.at[pl.ds(0, NZ - 1)], z_send)
         arrived(dall.at[:, pl.ds(0, (NFS - 1) * rk)], d_send)
         arrived(cb.at[pl.ds(0, 2 * NZ - 1)], c_send)
@@ -499,10 +508,10 @@
             pltpu.VMEM((2, rank // 2, 2 * tokens), F32),
             pltpu.VMEM((2, NFS, rk // 2, channels), F32),
             pltpu.VMEM((2, NFS, rk // 2, channels), BF16),
-            pltpu.VMEM((2, NFS, rk // 2, channels), BF16),
-            pltpu.VMEM((2, rk // 2, channels), F32),
-            pltpu.VMEM((2, rk // 2, channels), BF16),
-            pltpu.VMEM((2 * NZ, 2, rk // 2, width), BF16),
+            pltpu.VMEM((2, 2, NFS, rk // 2, channels), BF16),
+            pltpu.VMEM((2, 2, rk // 2, channels), F32),
+            pltpu.VMEM((2, 2, rk // 2, channels), BF16),
+            pltpu.VMEM((NZ, 2, 2, rk // 2, width), BF16),
             pltpu.VMEM((2, rank, width), BF16),
             pltpu.VMEM((2 * NZ, 2, width), F32),
             pltpu.VMEM((2, 2, *fm.shape), F32),
@@ -511,7 +520,7 @@
             dma((2,)),
         ]
         + [dma((2,)), dma((2, NX + NY - 2)), dma((2, NY))]
-        + [dma((2,))] * 2
+        + [dma((2,)), dma((2, 2))]
         + [dma] * 6
         + [dma((2,))]
         + [dma] * 4

time: 42.2 us -> 41.6 us (0.986)
  Pallas kernels: 41.4 us -> 40.9 us
    pallas_call x1, Pallas kernels: 40.5 us -> 39.9 us  [shards(): pl.pallas_call(functools.partial(kernel, sizes), out_shape=(small, small,...]
where the time goes in v7:
time: 41.6 us; the launch traced here: 41.5 us
  Pallas kernels  40.9 us (98%)
  between operations  0.64 us (2%)
    pallas_call x1, Pallas kernels, shards(): pl.pallas_call(functools.partial(kernel, sizes), out_shape=(small, small,...  39.9 us
    pallas_call x1, Pallas kernels, shards(): pl.pallas_call(store_kernel, out_shape=(small, small, block, block, block...  0.92 us

profile of v7, /device:TPU:1, one launch (start us, length us, event | category | flops | bytes accessed | tf_op | source)
XLA Modules:
  0.0 41.5 jit_solution(16815603459507866040)
XLA Ops:
  0.6 39.9 %shard_map.152 = (f32[16,2,64]{2,1,0:T(2,128)S(1)}, f32[16,2,64]{2,1,0:T(2,128)S(1)}, f32[64,128]{1,0:T(8,128)S(1)}, f32[64,128]{1,0:T(8,128)S(1)}, f32[64,128]{...) custom-call(bf16[256,2048]{1,0:T(8,128)(2,1)} %x_hbm.1, bf16[256,1024]{1,0:T(8,128)(2,1)} %g_hbm.1, ...), custom_call_target="tpu_custom_call" | custom-call | tf_op jit(solution)/shard_map/pallas_call | solution.py:494
  40.6 0.9 %shard_map.153 = (f32[16,2,64]{2,1,0:T(2,128)}, f32[16,2,64]{2,1,0:T(2,128)}, f32[64,128]{1,0:T(8,128)}, f32[64,128]{1,0:T(8,128)}, f32[64,128]{1,0:T(8,128)}, /...) custom-call(f32[16,2,64]{2,1,0:T(2,128)S(1)} %get-tuple-element.23.refs_0_, ...), custom_call_target="tpu_custom_call" | custom-call | tf_op jit(solution)/shard_map/pallas_call | solution.py:531

commit v8 on v7

--- a/solution.py
+++ b/solution.py
@@ -306,8 +306,8 @@
                 total = low[h, fs] if m else rs[0, h, 0].astype(F32)
                 for d in range(1, NFS):
                     total = total + rs[m, h, d].astype(F32)
+                psb[m, h] = total.astype(BF16)
                 psf[m, h] = total
-                psb[m, h] = total.astype(BF16)
 
     def z_copy(dz):
         zt = lax.rem(z + dz, NZ)
@@ -363,6 +363,7 @@
         for dz in range(1, NZ):
             for m in range(2):
                 wholes[m] = wholes[m] + zb[dz, m].astype(F32)
+        updated = []
         for m in range(2):
             part = wholes[m].reshape(rk, width)
             first_in = jnp.concatenate([fm[0, :, m, :], fm[1, :, m, :]], axis=1)
@@ -370,11 +371,13 @@
             first = BETA_FIRST * first_in + (1.0 - BETA_FIRST) * part
             second = BETA_SECOND * second_in + (1.0 - BETA_SECOND) * part * part
             dall[m, pl.ds(pl.multiple_of(fs * rk, rk), rk), :] = (first / jnp.sqrt(second)).astype(BF16)
-            for i in range(2):
-                fx[i, 0, :, m, :] = first[:, i * half : (i + 1) * half]
-                fx[i, 1, :, m, :] = second[:, i * half : (i + 1) * half]
+            updated.append((first, second))
         for d in fs_offsets:
             d_copy(d).start()
+        for m in range(2):
+            for k in range(2):
+                for i in range(2):
+                    fx[i, k, :, m, :] = updated[m][k][:, i * half : (i + 1) * half]
         back_copies[0].start()
 
     pl.when(c == 1)(m_onward)

time: 41.6 us -> 41.5 us (level)
  no operation moved by 1% of the time
where the time goes in v8:
time: 41.5 us; the launch traced here: 41.4 us
  Pallas kernels  40.7 us (98%)
  between operations  0.64 us (2%)
    pallas_call x1, Pallas kernels, shards(): pl.pallas_call(functools.partial(kernel, sizes), out_shape=(small, small,...  39.8 us
    pallas_call x1, Pallas kernels, shards(): pl.pallas_call(store_kernel, out_shape=(small, small, block, block, block...  0.92 us

profile of v8, /device:TPU:1, one launch (start us, length us, event | category | flops | bytes accessed | tf_op | source)
XLA Modules:
  0.0 41.4 jit_solution(7391378945493282477)
XLA Ops:
  0.6 39.8 %shard_map.152 = (f32[16,2,64]{2,1,0:T(2,128)S(1)}, f32[16,2,64]{2,1,0:T(2,128)S(1)}, f32[64,128]{1,0:T(8,128)S(1)}, f32[64,128]{1,0:T(8,128)S(1)}, f32[64,128]{...) custom-call(bf16[256,2048]{1,0:T(8,128)(2,1)} %x_hbm.1, bf16[256,1024]{1,0:T(8,128)(2,1)} %g_hbm.1, ...), custom_call_target="tpu_custom_call" | custom-call | tf_op jit(solution)/shard_map/pallas_call | solution.py:497
  40.5 0.9 %shard_map.153 = (f32[16,2,64]{2,1,0:T(2,128)}, f32[16,2,64]{2,1,0:T(2,128)}, f32[64,128]{1,0:T(8,128)}, f32[64,128]{1,0:T(8,128)}, f32[64,128]{1,0:T(8,128)}, /...) custom-call(f32[16,2,64]{2,1,0:T(2,128)S(1)} %get-tuple-element.23.refs_0_, ...), custom_call_target="tpu_custom_call" | custom-call | tf_op jit(solution)/shard_map/pallas_call | solution.py:534
